TPU v7x, 128 devices: a whole 4x4x4 slice. The times are simulated.
128 devices in a mesh: sp: 16 (over z, x), dp: 8 (over y, core).
Axes of the slice: x: 4, y: 4, z: 4, core: 2. Of those that a mesh axis runs over, the one named last changes fastest.
Arguments:
- tokens: bfloat16 [8, 6144, 2048], P('dp', 'sp'), may hold values from -6 to 6
- q_weight: bfloat16 [2048, 1024], P(('sp', 'dp')), may hold values from -0.13258252 to 0.13258252
- k_weight: bfloat16 [2048, 256], P(('sp', 'dp')), may hold values from -0.13258252 to 0.13258252
- v_weight: bfloat16 [2048, 256], P(('sp', 'dp')), may hold values from -0.125 to 0.125
- out_weight: bfloat16 [1024, 2048], P(None, ('sp', 'dp')), may hold values from -6 to 6
- q_gain: float32 [64], replicated, may hold values from 0.5 to 8
- k_gain: float32 [64], replicated, may hold values from 0.5 to 8
Outputs:
- mixed: bfloat16 [8, 6144, 2048], P('dp', 'sp')
All inputs are finite; a program needn't handle non-finite values.
Results may differ from a plain program's by a relative error of at most 0.0055.
The roundings to bfloat16 on the way count: a program that leaves them out, or rounds other values in their place, can miss the bound.
Values may be sent and summed in bfloat16 or wider, within the bound.
No kernel may reach another device: no remote copies, remote signals or barrier semaphores. Data moves between devices by JAX's collectives and lax.ppermute only.
A program may use at most 128 MiB of HBM per device.

v0:
```python
import jax
import jax.numpy as jnp
import numpy as np
from jax import lax
from jax.experimental import pallas as pl
from jax.experimental.pallas import tpu as pltpu
from jax.sharding import PartitionSpec as P

GRID_W = 64
LOG2E = 1.4426950408889634
V_ROWS = 80
ATTEND_VMEM = 24 * 2**20
HEAD = 64
KV_HEADS = 4
GROUP = 4
TOK = 384
WIDE = 384
QKV = KV_HEADS * WIDE
OUT_IN = 1024
MODEL = 2048

epsilon = 1e-06
rope_base = 10000.0

AXES = ("sp", "dp")
DEVICE = np.arange(128).reshape(4, 4, 4, 2)
SHIFTS = (0, -1, 1, 2)


def lines(axis, core):
    return np.moveaxis(DEVICE[..., core], "zxy".index(axis), -1).reshape(-1, 4).tolist()


def shift_pairs(axis_of_core, step):
    pairs = []
    for core, axis in enumerate(axis_of_core):
        for line in lines(axis, core):
            pairs += [(line[i], line[(i + step) % 4]) for i in range(4)]
    return pairs


INNER = ("x", "z")
OUTER = ("z", "x")
SWAP = [(int(i), int(i) ^ 1) for i in range(128)]
EXCHANGE = lines("x", 0) + lines("z", 1)


def shift(array, axis_of_core, step):
    return lax.ppermute(array, AXES, shift_pairs(axis_of_core, step))


def pair(array, axis_of_core, far):
    pairs = []
    for core, axis in enumerate(axis_of_core):
        for line in lines(axis, core):
            pairs += [(line[i], line[3 - i if far else i ^ 1]) for i in range(4)]
    return lax.ppermute(array, AXES, pairs)


def swap(array):
    return lax.ppermute(array, AXES, SWAP)


def ring(top, bottom, axis_of_core):
    left_top = shift(top, axis_of_core, 1)
    right_bottom = shift(bottom, axis_of_core, -1)
    left_bottom = shift(bottom, axis_of_core, 1)
    right_top = shift(top, axis_of_core, -1)
    far_top = shift(left_top, axis_of_core, 1)
    far_bottom = shift(right_bottom, axis_of_core, -1)
    return left_top, left_bottom, right_top, right_bottom, far_top, far_bottom


def ring_order(at):
    return [(at + s + 4) % 4 for s in SHIFTS]


def pair_order(at):
    near = at + 1 - 2 * (at % 2)
    return [at, near, 3 - at, 3 - near]


def lay_out(where, mine, theirs, full_ref, outer_order):
    z, x, y, own_core = where
    y_at = ring_order(y)
    for pieces, core in ((mine, own_core), (theirs, 1 - own_core)):
        first = core == 0
        outer_at = outer_order(jnp.where(first, z, x))
        inner_at = ring_order(jnp.where(first, x, z))
        stack = [(p, r) for p in pieces for r in range(0, p.shape[0], 16)]
        for outer in range(4):
            for inner in range(4):
                z_at = jnp.where(first, outer_at[outer], inner_at[inner])
                x_at = jnp.where(first, inner_at[inner], outer_at[outer])
                base = (z_at * 4 + x_at) * 128 + core * 16
                for step in range(4):
                    source, row = stack[outer * 16 + inner * 4 + step]
                    at = pl.multiple_of(base + y_at[step] * 32, 16)
                    full_ref[pl.ds(at, 16), :] = source[row : row + 16, :]


def column(row):
    size = row.shape[1]
    diagonal = lax.broadcasted_iota(jnp.int32, (size, size), 0) == lax.broadcasted_iota(
        jnp.int32, (size, size), 1
    )
    return jnp.sum(jnp.where(diagonal, row, 0.0), axis=1, keepdims=True)


def project(where, tokens, mine, theirs, tables, q_gain, k_gain):
    count = len(mine)

    def kern(where_ref, tok_ref, *refs):
        table_ref, qg_ref, kg_ref, out_ref, full_ref = refs[2 * count :]
        place = [where_ref[i] for i in range(4)]
        lay_out(place, refs[:count], refs[count : 2 * count], full_ref, ring_order)
        cos_r, sin_r = table_ref[0:16, :], table_ref[16:32, :]
        cos_c, sin_c = table_ref[32:48, :], table_ref[48:64, :]
        gains = (column(qg_ref[...]), column(kg_ref[...]))
        tok = tok_ref[...]
        heads = GROUP * KV_HEADS
        for pair in range((heads + 2 * KV_HEADS) // 2):
            cols = slice(pair * 2 * HEAD, (pair + 1) * 2 * HEAD)
            if pair % 2 == 0:
                both = slice(cols.start, cols.start + 4 * HEAD)
                raw = jnp.dot(tok, full_ref[:, both], preferred_element_type=jnp.float32)
            flat = raw[:, (pair % 2) * 2 * HEAD : (pair % 2 + 1) * 2 * HEAD].T
            for i in range(2):
                head = 2 * pair + i
                v = flat[i * HEAD : (i + 1) * HEAD, :]
                if head < heads + KV_HEADS:
                    mean_sq = jnp.mean(v * v, axis=0, keepdims=True)
                    v = v * lax.rsqrt(mean_sq + epsilon) * gains[head // heads]
                    a, b, c, d = v[0:16], v[16:32], v[32:48], v[48:64]
                    v = jnp.concatenate(
                        [
                            a * cos_r - b * sin_r,
                            b * cos_r + a * sin_r,
                            c * cos_c - d * sin_c,
                            d * cos_c + c * sin_c,
                        ],
                        axis=0,
                    )
                if head < heads:
                    group, at = head // GROUP, head % GROUP
                else:
                    group, at = head % KV_HEADS, GROUP + (head - heads) // KV_HEADS
                out_ref[group, at * HEAD : (at + 1) * HEAD, :] = v.astype(jnp.bfloat16)

    return pl.pallas_call(
        kern,
        in_specs=[pl.BlockSpec(memory_space=pltpu.SMEM)]
        + [pl.BlockSpec(memory_space=pltpu.VMEM)] * (2 * count + 4),
        out_specs=pl.BlockSpec(memory_space=pltpu.VMEM),
        out_shape=jax.ShapeDtypeStruct((KV_HEADS, WIDE, TOK), jnp.bfloat16),
        scratch_shapes=[pltpu.VMEM((MODEL, QKV), jnp.bfloat16)],
        compiler_params=pltpu.CompilerParams(vmem_limit_bytes=28 * 2**20),
        cost_estimate=pl.CostEstimate(
            flops=2 * TOK * MODEL * QKV, bytes_accessed=2 * MODEL * QKV, transcendentals=0
        ),
        name="project",
    )(where, tokens, *mine, *theirs, tables, q_gain, k_gain)


def attend(place, q_gain, k_gain, qkv, pieces, before, last):
    keys = sum(p.shape[0] for p in pieces) * TOK
    places = place.shape[0]
    tile = 256
    block = 512
    ahead = 2
    wide = GROUP * TOK
    more = before is not None

    def kern(place_ref, qg_ref, kg_ref, q_ref, *refs):
        sources = refs[: len(pieces)]
        rest = refs[len(pieces) :]
        if more:
            acc_in, top_in = rest[:2]
            rest = rest[2:]
        *outs, k_ref, v_ref = rest

        @pl.when(pl.program_id(0) == 0)
        def _():
            at = 0
            for source in sources:
                for i in range(source.shape[0]):
                    k = source[i, 0:HEAD, :]
                    k_ref[at : at + TOK, :] = jnp.concatenate([k, k], axis=0).T
                    v_ref[0:HEAD, at : at + TOK] = source[i, HEAD : 2 * HEAD, :]
                    at += TOK
            row = lax.broadcasted_iota(jnp.int32, (V_ROWS - HEAD, keys), 0)
            v_ref[HEAD:, :] = jnp.where(row == 0, 1.0, 0.0).astype(jnp.bfloat16)

        q = jnp.concatenate([q_ref[0, h * HEAD : (h + 1) * HEAD, :] for h in range(GROUP)], axis=1)
        limit = 8.0 * jnp.max(jnp.abs(qg_ref[...])) * jnp.max(jnp.abs(kg_ref[...]))

        def finish(acc, top):
            if not last:
                outs[0][0] = acc
                outs[1][0] = top
                return
            result = (acc[:HEAD] / acc[HEAD : HEAD + 1]).astype(jnp.bfloat16)
            for n in range(places):

                @pl.when(pl.program_id(0) == n)
                def _():
                    for h in range(GROUP):
                        outs[n][h * HEAD : (h + 1) * HEAD, :] = result[:, h * TOK : (h + 1) * TOK]

        @pl.when(limit <= 60.0)
        def _():
            scaled = q.astype(jnp.float32) * (0.125 * LOG2E)
            high = scaled.astype(jnp.bfloat16)
            low = (scaled - high.astype(jnp.float32)).astype(jnp.bfloat16)
            q2 = jnp.concatenate([high, low], axis=0)
            work = [(b, u) for b in range(0, wide, block) for u in range(0, keys, tile)]

            def score(item):
                b, u = item
                return jnp.dot(
                    k_ref[u : u + tile, :], q2[:, b : b + block], preferred_element_type=jnp.float32
                )

            waiting = [score(item) for item in work[:ahead]]
            done = []
            for n, (b, u) in enumerate(work):
                if n + ahead < len(work):
                    waiting.append(score(work[n + ahead]))
                if u == 0 and more:
                    acc = acc_in[0, :, b : b + block]
                elif u == 0:
                    acc = jnp.zeros((V_ROWS, block), jnp.float32)
                weights = jnp.exp2(waiting.pop(0)).astype(jnp.bfloat16)
                acc = acc + jnp.dot(
                    v_ref[:, u : u + tile], weights, preferred_element_type=jnp.float32
                )
                if u + tile == keys:
                    done.append(acc)
            finish(jnp.concatenate(done, axis=1), jnp.zeros((8, wide), jnp.float32))

        @pl.when(jnp.logical_not(limit <= 60.0))
        def _():
            step_rows = 512

            def step(u, carry):
                top, acc = carry
                rows = pl.ds(pl.multiple_of(u * step_rows, step_rows), step_rows)
                scores = (
                    jnp.dot(k_ref[rows, :HEAD], q, preferred_element_type=jnp.float32) * 0.125
                )
                new_top = jnp.maximum(top, jnp.max(scores, axis=0, keepdims=True))
                weights = jnp.exp(scores - new_top).astype(jnp.bfloat16)
                part = jnp.dot(v_ref[:, rows], weights, preferred_element_type=jnp.float32)
                return new_top, acc * jnp.exp(top - new_top) + part

            if more:
                start = (top_in[0, 0:1, :], acc_in[0])
            else:
                start = (
                    jnp.full((1, wide), -1e30, jnp.float32),
                    jnp.zeros((V_ROWS, wide), jnp.float32),
                )
            top, acc = lax.fori_loop(0, keys // step_rows, step, start)
            finish(acc, jnp.broadcast_to(top, (8, wide)))

    def whole(array, at):
        return pl.BlockSpec((array.shape[0], 2 * HEAD, TOK), lambda n, place: (0, at, 0))

    sums = [
        pl.BlockSpec((1, V_ROWS, wide), lambda n, place: (place[n], 0, 0)),
        pl.BlockSpec((1, 8, wide), lambda n, place: (place[n], 0, 0)),
    ]
    gain = pl.BlockSpec((1, HEAD), lambda n, place: (0, 0))
    result = pl.BlockSpec((GROUP * HEAD, TOK), lambda n, place: (0, 0))
    return pl.pallas_call(
        kern,
        grid_spec=pltpu.PrefetchScalarGridSpec(
            num_scalar_prefetch=1,
            grid=(places,),
            in_specs=[
                gain,
                gain,
                pl.BlockSpec((1, GROUP * HEAD, TOK), lambda n, place: (place[n], 0, 0)),
                *[whole(p, 0 if p.shape[1] == 2 * HEAD else 2) for p in pieces],
                *(sums if more else []),
            ],
            out_specs=[result] * places if last else sums,
            scratch_shapes=[
                pltpu.VMEM((keys, 2 * HEAD), jnp.bfloat16),
                pltpu.VMEM((V_ROWS, keys), jnp.bfloat16),
            ],
        ),
        out_shape=[jax.ShapeDtypeStruct((GROUP * HEAD, TOK), jnp.bfloat16)] * places
        if last
        else [
            jax.ShapeDtypeStruct((4, V_ROWS, wide), jnp.float32),
            jax.ShapeDtypeStruct((4, 8, wide), jnp.float32),
        ],
        compiler_params=pltpu.CompilerParams(vmem_limit_bytes=ATTEND_VMEM),
        cost_estimate=pl.CostEstimate(
            flops=4 * places * keys * wide * 256 * 2,
            bytes_accessed=2 * keys * 2 * HEAD,
            transcendentals=places * keys * wide,
        ),
    )(place, q_gain, k_gain, qkv, *pieces, *(before or []))


def mix(where, attended, mine, theirs):
    count = len(mine)

    def kern(where_ref, *refs):
        heads = refs[:4]
        refs = refs[4:]
        out_ref, full_ref, att_ref = refs[2 * count :]
        place = [where_ref[i] for i in range(4)]
        lay_out(place, refs[:count], refs[count : 2 * count], full_ref, pair_order)
        groups = ring_order(jnp.where(place[3] == 0, place[1], place[0]))
        for group, source in zip(groups, heads):
            at = pl.multiple_of(group * GROUP * HEAD, GROUP * HEAD)
            att_ref[pl.ds(at, GROUP * HEAD), :] = source[...]
        rows = att_ref[...].T
        out_ref[...] = lax.dot_general(
            rows, full_ref[...], (((1,), (1,)), ((), ())), preferred_element_type=jnp.float32
        ).astype(jnp.bfloat16)

    def piece(array):
        return pl.BlockSpec(array.shape, lambda: (0, 0))

    return pl.pallas_call(
        kern,
        in_specs=[
            pl.BlockSpec(memory_space=pltpu.SMEM),
            *[piece(a) for a in attended],
            *[piece(a) for a in mine],
            *[piece(a) for a in theirs],
        ],
        out_specs=pl.BlockSpec((TOK, MODEL), lambda: (0, 0)),
        out_shape=jax.ShapeDtypeStruct((TOK, MODEL), jnp.bfloat16),
        scratch_shapes=[
            pltpu.VMEM((MODEL, OUT_IN), jnp.bfloat16),
            pltpu.VMEM((OUT_IN, TOK), jnp.bfloat16),
        ],
        compiler_params=pltpu.CompilerParams(vmem_limit_bytes=24 * 2**20),
        cost_estimate=pl.CostEstimate(
            flops=2 * TOK * MODEL * OUT_IN, bytes_accessed=2 * MODEL * OUT_IN, transcendentals=0
        ),
        name="mix",
    )(where, *attended, *mine, *theirs)


def rotation_tables(offset):
    quarter = HEAD // 4
    positions = jnp.arange(TOK, dtype=jnp.int32) + offset
    frequency = rope_base ** (-jnp.arange(quarter, dtype=jnp.float32) / quarter)
    parts = []
    for coords in (positions // GRID_W, positions % GRID_W):
        angles = coords.astype(jnp.float32)[None, :] * frequency[:, None]
        parts += [jnp.cos(angles), jnp.sin(angles)]
    return jnp.concatenate(parts, axis=0)


def per_device(tokens, q_weight, k_weight, v_weight, out_weight, q_gain, k_gain):
    sp = lax.axis_index("sp")
    dp = lax.axis_index("dp")
    where = jnp.stack([sp // 4, sp % 4, dp // 2, dp % 2]).astype(jnp.int32)
    tables = rotation_tables(sp * TOK)
    q_row = q_gain.reshape(1, HEAD)
    k_row = k_gain.reshape(1, HEAD)

    own = jnp.concatenate([q_weight, k_weight, v_weight, out_weight.T], axis=1)
    block = jnp.concatenate([own, *[shift(own, ("y", "y"), -s) for s in SHIFTS[1:]]], axis=0)
    left = shift(block, INNER, 1)
    right = shift(block, INNER, -1)
    middle = block.shape[0] // 2
    far_top = shift(left[:middle], INNER, 1)
    far_bottom = shift(right[middle:], INNER, -1)
    half = jnp.concatenate([block, left], axis=0)
    other = jnp.concatenate([right, far_top, far_bottom], axis=0)
    tables, where, half, other = lax.optimization_barrier((tables, where, half, other))

    in_mine = [half[:, :QKV], other[:, :QKV]]
    in_mine += ring(*in_mine, OUTER)
    in_theirs = [swap(a) for a in in_mine]
    qkv = project(where, tokens[0], in_mine, in_theirs, tables, q_row, k_row)

    out_own = jnp.concatenate([half[:, QKV:], other[:, QKV:]], axis=0)
    qkv, out_own = lax.optimization_barrier(
        (
            lax.all_to_all(
                qkv, AXES, split_axis=0, concat_axis=0, tiled=True, axis_index_groups=EXCHANGE
            ),
            out_own,
        )
    )
    every = jnp.arange(4, dtype=jnp.int32)
    here = jnp.where(dp % 2 == 0, sp % 4, sp // 4).astype(jnp.int32)
    away = jnp.stack(ring_order(here)[1:])
    kv_own = qkv[:, GROUP * HEAD :, :]
    kv_near = pair(kv_own, OUTER, False)
    out_near = pair(out_own, OUTER, False)
    sums = attend(every, q_row, k_row, qkv, [qkv], None, False)
    sums, kv_own, kv_near = lax.optimization_barrier((sums, kv_own, kv_near))
    kv_other = pair(jnp.concatenate([kv_own, kv_near], axis=0), OUTER, True)
    sums = attend(every, q_row, k_row, qkv, [kv_near], sums, False)
    sums, kv_other, out_near = lax.optimization_barrier((sums, kv_other, out_near))
    out_half = jnp.concatenate([out_own, out_near], axis=0)
    out_other = pair(out_half, OUTER, True)
    out_half_theirs = swap(out_half)
    behind, ahead, across = attend(away, q_row, k_row, qkv, [kv_other], sums, True)
    sums, kv_other, behind, ahead, across, out_half_theirs = lax.optimization_barrier(
        (sums, kv_other, behind, ahead, across, out_half_theirs)
    )
    across = shift(across, INNER, 2)
    ahead = shift(ahead, INNER, 1)
    behind = shift(behind, INNER, -1)
    (own,) = attend(here.reshape(1), q_row, k_row, qkv, [kv_other], sums, True)
    own, out_other = lax.optimization_barrier((own, out_other))
    out_other_theirs = swap(out_other)
    return mix(
        where, [own, ahead, behind, across], [out_half, out_other], [out_half_theirs, out_other_theirs]
    )[None]


def solution(mesh):
    return jax.shard_map(
        per_device,
        mesh=mesh,
        in_specs=(
            P("dp", "sp", None),
            P(("sp", "dp"), None),
            P(("sp", "dp"), None),
            P(("sp", "dp"), None),
            P(None, ("sp", "dp")),
            P(),
            P(),
        ),
        out_specs=P("dp", "sp", None),
        check_vma=False,
    )
```

profile of v0, /device:TPU:0, one launch (start us, length us, event | category | flops | bytes accessed | tf_op | source)
XLA Modules:
  0.0 171.2 jit_solution(4271024779668789755)
XLA Ops:
  0.0 0.8 pad_maximum_fusion.5
  0.8 3.2 %collective-permute-start.1 = (bf16[16,2560]{1,0:T(8,128)(2,1)S(1)}, bf16[16,2560]{1,0:T(8,128)(2,1)S(1)}, u32[]{:S(2)}, u32[]{:S(2)}) collective-permute-start(bf16[16,2560]{1,0:T(8,128)(2,1)S(1)} %get-tuple-element.65), channel_id=1, source_target_pairs={{0,6},{2,0},{4,2},{6,4},{8,14},{10,8},{12,10},{14,12},{16,22},{18,... | collective-permute-start | bytes 245768 | tf_op jit(solution)/shard_map/ppermute | solution.py:49
  4.0 2.2 %collective-permute-start.2 = (bf16[16,2560]{1,0:T(8,128)(2,1)S(1)}, bf16[16,2560]{1,0:T(8,128)(2,1)S(1)}, u32[]{:S(2)}, u32[]{:S(2)}) collective-permute-start(bf16[16,2560]{1,0:T(8,128)(2,1)S(1)} %get-tuple-element.65), channel_id=1, source_target_pairs={{0,4},{2,6},{4,0},{6,2},{8,12},{10,14},{12,8},{14,10},{16,20},{18,... | collective-permute-start | bytes 245768 | tf_op jit(solution)/shard_map/ppermute | solution.py:49
  6.6 4.3 %collective-permute-done = bf16[16,2560]{1,0:T(8,128)(2,1)S(1)} collective-permute-done((bf16[16,2560]{1,0:T(8,128)(2,1)S(1)}, bf16[16,2560]{1,0:T(8,128)(2,1)S(1)}, u32[]{:S(2)}, u32[]{:S(2)}) %collective-permute-start) | collective-permute-done | bytes 81952 | tf_op jit(solution)/shard_map/ppermute | solution.py:49
  10.9 0.8 pad_maximum_fusion.3
  11.7 2.8 %collective-permute-start.4 = (bf16[64,2560]{1,0:T(8,128)(2,1)S(1)}, bf16[64,2560]{1,0:T(8,128)(2,1)S(1)}, u32[]{:S(2)}, u32[]{:S(2)}) collective-permute-start(bf16[64,2560]{1,0:T(8,128)(2,1)S(1)} %pad_maximum_fusion.3), channel_id=1, source_target_pairs={{0,24},{8,0},{16,8},{24,16},{2,26},{10,2},{18,10},{26,18},{4,28},{... | collective-permute-start | bytes 983048 | tf_op jit(solution)/shard_map/ppermute | solution.py:49
  14.6 4.5 %collective-permute-done.4 = bf16[64,2560]{1,0:T(8,128)(2,1)S(1)} collective-permute-done((bf16[64,2560]{1,0:T(8,128)(2,1)S(1)}, bf16[64,2560]{1,0:T(8,128)(2,1)S(1)}, u32[]{:S(2)}, u32[]{:S(2)}) %collective-permute-start.4) | collective-permute-done | bytes 327712 | tf_op jit(solution)/shard_map/ppermute | solution.py:49
  19.2 3.8 %collective-permute-start.6 = (bf16[32,2560]{1,0:T(8,128)(2,1)S(1)}, bf16[32,2560]{1,0:T(8,128)(2,1)S(1)}, u32[]{:S(2)}, u32[]{:S(2)}) collective-permute-start(bf16[32,2560]{1,0:T(8,128)(2,1)S(1)} %slice.29), channel_id=1, source_target_pairs={{0,24},{8,0},{16,8},{24,16},{2,26},{10,2},{18,10},{26,18},{4,28},{... | collective-permute-start | bytes 491528 | tf_op jit(solution)/shard_map/ppermute | solution.py:49
  23.1 2.7 %collective-permute-done.6 = bf16[32,2560]{1,0:T(8,128)(2,1)S(1)} collective-permute-done((bf16[32,2560]{1,0:T(8,128)(2,1)S(1)}, bf16[32,2560]{1,0:T(8,128)(2,1)S(1)}, u32[]{:S(2)}, u32[]{:S(2)}) %collective-permute-start.6) | collective-permute-done | bytes 163872 | tf_op jit(solution)/shard_map/ppermute | solution.py:49
  25.8 3.8 %collective-permute-done.5 = bf16[32,2560]{1,0:T(8,128)(2,1)S(1)} collective-permute-done((bf16[32,2560]{1,0:T(8,128)(2,1)S(1)}, bf16[32,2560]{1,0:T(8,128)(2,1)S(1)}, u32[]{:S(2)}, u32[]{:S(2)}) %collective-permute-start.5) | collective-permute-done | bytes 163872 | tf_op jit(solution)/shard_map/ppermute | solution.py:49
  29.7 4.1 %collective-permute-start.10 = (bf16[128,1536]{1,0:T(8,128)(2,1)S(1)}, bf16[128,1536]{1,0:T(8,128)(2,1)S(1)}, u32[]{:S(2)}, u32[]{:S(2)}) collective-permute-start(bf16[128,1536]{1,0:T(8,128)(2,1)S(1)} %slice.24.refs_1_), channel_id=1, source_target_pairs={{0,96},{32,0},{64,32},{96,64},{2,98},{34,2},{66,34},{98,66},{4,100... | collective-permute-start | bytes 1179656 | tf_op jit(solution)/shard_map/ppermute | solution.py:49
  34.0 3.3 %collective-permute-start.9 = (bf16[128,1536]{1,0:T(8,128)(2,1)S(1)}, bf16[128,1536]{1,0:T(8,128)(2,1)S(1)}, u32[]{:S(2)}, u32[]{:S(2)}) collective-permute-start(bf16[128,1536]{1,0:T(8,128)(2,1)S(1)} %slice.23.refs_0_), channel_id=1, source_target_pairs={{0,96},{32,0},{64,32},{96,64},{2,98},{34,2},{66,34},{98,66},{4,100... | collective-permute-start | bytes 1179656 | tf_op jit(solution)/shard_map/ppermute | solution.py:49
  37.3 1.8 %collective-permute-done.10.refs_5_ = bf16[128,1536]{1,0:T(8,128)(2,1)S(1)} collective-permute-done((bf16[128,1536]{1,0:T(8,128)(2,1)S(1)}, bf16[128,1536]{1,0:T(8,128)(2,1)S(1)}, u32[]{:S(2)}, u32[]{:S(2)}) %collective-permute-start.10) | collective-permute-done | bytes 393248 | tf_op jit(solution)/shard_map/ppermute | solution.py:49
  39.1 3.7 %collective-permute-done.8.refs_3_ = bf16[128,1536]{1,0:T(8,128)(2,1)S(1)} collective-permute-done((bf16[128,1536]{1,0:T(8,128)(2,1)S(1)}, bf16[128,1536]{1,0:T(8,128)(2,1)S(1)}, u32[]{:S(2)}, u32[]{:S(2)}) %collective-permute-start.8) | collective-permute-done | bytes 393248 | tf_op jit(solution)/shard_map/ppermute | solution.py:49
  42.8 4.2 %collective-permute-done.7.refs_2_ = bf16[128,1536]{1,0:T(8,128)(2,1)S(1)} collective-permute-done((bf16[128,1536]{1,0:T(8,128)(2,1)S(1)}, bf16[128,1536]{1,0:T(8,128)(2,1)S(1)}, u32[]{:S(2)}, u32[]{:S(2)}) %collective-permute-start.7) | collective-permute-done | bytes 393248 | tf_op jit(solution)/shard_map/ppermute | solution.py:49
  47.6 2.9 %collective-permute-done.12.refs_7_ = bf16[128,1536]{1,0:T(8,128)(2,1)S(1)} collective-permute-done((bf16[128,1536]{1,0:T(8,128)(2,1)S(1)}, bf16[128,1536]{1,0:T(8,128)(2,1)S(1)}, u32[]{:S(2)}, u32[]{:S(2)}) %collective-permute-start.12) | collective-permute-done | bytes 393248 | tf_op jit(solution)/shard_map/ppermute | solution.py:49
  50.6 5.4 %collective-permute-done.11.refs_6_ = bf16[128,1536]{1,0:T(8,128)(2,1)S(1)} collective-permute-done((bf16[128,1536]{1,0:T(8,128)(2,1)S(1)}, bf16[128,1536]{1,0:T(8,128)(2,1)S(1)}, u32[]{:S(2)}, u32[]{:S(2)}) %collective-permute-start.11) | collective-permute-done | bytes 393248 | tf_op jit(solution)/shard_map/ppermute | solution.py:49
  56.0 1.7 collective-permute-done.19.refs_14_
  57.8 4.9 %project.1 = bf16[4,384,384]{2,1,0:T(8,128)(2,1)} custom-call(s32[4]{0:T(128)S(1)} %pad_add_fusion.where_ref, bf16[384,2048]{1,0:T(8,128)(2,1)S(1)} %bitcast.13, bf16[128,1536]{1,0:T(8,128)(2,1)S(1)} %slice.23.refs_0_, bf16[128,1536]{1,0:T(8,128)(2,1)S(1)} %slice.24.refs_1_, bf16[128,1536]{1,0:T(8,128)(2,1)S(1)} %collective-permute-done.7.refs_2_, ...), custom_call_target="tpu_custom_call" | custom-call | flops 2415919104 | bytes 6291456 | tf_op jit(solution)/shard_map/project/pallas_call | solution.py:150
  62.6 3.5 %all-to-all-start = ((bf16[4,384,384]{2,1,0:T(8,128)(2,1)}), bf16[4,384,384]{2,1,0:T(8,128)(2,1)S(1)}, u32[]{:S(2)}, u32[]{:S(2)}) async-start(bf16[4,384,384]{2,1,0:T(8,128)(2,1)} %project.1), calls=%async_computation | async-start | bytes 2359296 | tf_op jit(solution)/shard_map/all_to_all | solution.py:389
  66.4 11.3 %all-to-all-done.q_ref.refs_0_ = bf16[4,384,384]{2,1,0:T(8,128)(2,1)S(1)} async-done(((bf16[4,384,384]{2,1,0:T(8,128)(2,1)}), bf16[4,384,384]{2,1,0:T(8,128)(2,1)S(1)}, u32[]{:S(2)}, u32[]{:S(2)}) %all-to-all-start) | async-done | bytes 1179680 | tf_op jit(solution)/shard_map/all_to_all | solution.py:389
  77.9 2.0 %collective-permute-start.23 = (bf16[256,1024]{1,0:T(8,128)(2,1)S(1)}, bf16[256,1024]{1,0:T(8,128)(2,1)S(1)}, u32[]{:S(2)}, u32[]{:S(2)}) collective-permute-start(bf16[256,1024]{1,0:T(8,128)(2,1)S(1)} %pad_maximum_fusion.2), channel_id=1, source_target_pairs={{0,32},{32,0},{64,96},{96,64},{2,34},{34,2},{66,98},{98,66},{4,36}... | collective-permute-start | bytes 1572872 | tf_op jit(solution)/shard_map/ppermute | solution.py:57
  79.9 18.5 %shard_map.73 = (f32[4,80,1536]{2,1,0:T(8,128)S(1)}, f32[4,8,1536]{2,1,0:T(8,128)S(1)}) custom-call(s32[4]{0:T(128)S(1)} %iota.22.place_ref, f32[1,64]{1,0:T(1,128)S(1)} %bitcast.15, f32[1,64]{1,0:T(1,128)S(1)} %bitcast.20, bf16[4,384,384]{2,1,0:T(8,128)(2,1)S(1)} %all-to-all-done.q_ref.refs_0_, bf16[4,384,384]{2,1,0:T(8,128)(2,1)S(1)} %all-to-all-done.q_ref.refs_0_), custom_call_target="tpu_custom_call" | custom-call | flops 19327352832 | bytes 393216 | tf_op jit(solution)/shard_map/pallas_call | solution.py:275
  98.7 18.6 %shard_map.74 = (f32[4,80,1536]{2,1,0:T(8,128)S(1)}, f32[4,8,1536]{2,1,0:T(8,128)S(1)}) custom-call(s32[4]{0:T(128)S(1)} %iota.21.place_ref, f32[1,64]{1,0:T(1,128)S(1)} %bitcast.16, f32[1,64]{1,0:T(1,128)S(1)} %bitcast.21, bf16[4,384,384]{2,1,0:T(8,128)(2,1)S(1)} %all-to-all-done.q_ref.refs_0_, bf16[4,128,384]{2,1,0:T(8,128)(2,1)S(1)} %collective-permute-done.21.refs_0_, ...), custom_call_target="tpu_custom_call" | custom-call | flops 19327352832 | bytes 393216 | tf_op jit(solution)/shard_map/pallas_call | solution.py:275
  117.3 3.3 %collective-permute-start.25 = (bf16[512,1024]{1,0:T(8,128)(2,1)S(1)}, bf16[512,1024]{1,0:T(8,128)(2,1)S(1)}, u32[]{:S(2)}, u32[]{:S(2)}) collective-permute-start(bf16[512,1024]{1,0:T(8,128)(2,1)S(1)} %constant_dynamic-update-slice_fusion.5.refs_4_), channel_id=1, source_target_pairs={{0,96},{32,64},{64,32},{96,0},{2,98},{34,66},{66,34},{98,2},{4,100... | collective-permute-start | bytes 3145736 | tf_op jit(solution)/shard_map/ppermute | solution.py:57
  120.6 26.9 %shard_map.75 = (bf16[256,384]{1,0:T(8,128)(2,1)S(1)}, bf16[256,384]{1,0:T(8,128)(2,1)S(1)}, bf16[256,384]{1,0:T(8,128)(2,1)S(1)}) custom-call(s32[3]{0:T(128)S(1)} %pad_add_fusion.1.place_ref, f32[1,64]{1,0:T(1,128)S(1)} %bitcast.17, f32[1,64]{1,0:T(1,128)S(1)} %bitcast.22, bf16[4,384,384]{2,1,0:T(8,128)(2,1)S(1)} %all-to-all-done.q_ref.refs_0_, ...), custom_call_target="tpu_custom_call" | custom-call | flops 28991029248 | bytes 786432 | tf_op jit(solution)/shard_map/pallas_call | solution.py:275
  147.5 8.8 %shard_map.76.refs_0_ = bf16[256,384]{1,0:T(8,128)(2,1)S(1)} custom-call(s32[1]{0:T(128)} %bitcast.5.place_ref, f32[1,64]{1,0:T(1,128)S(1)} %bitcast.18, f32[1,64]{1,0:T(1,128)S(1)} %bitcast.23, bf16[4,384,384]{2,1,0:T(8,128)(2,1)S(1)} %all-to-all-done.q_ref.refs_0_, bf16[8,128,384]{2,1,0:T(8,128)(2,1)S(1)} %collective-permute-done.22.refs_0_, ...), custom_call_target="tpu_custom_call" | custom-call | flops 9663676416 | bytes 786432 | tf_op jit(solution)/shard_map/pallas_call | solution.py:275
  157.5 2.7 %collective-permute-start.27 = (bf16[256,384]{1,0:T(8,128)(2,1)S(1)}, bf16[256,384]{1,0:T(8,128)(2,1)S(1)}, u32[]{:S(2)}, u32[]{:S(2)}) collective-permute-start(bf16[256,384]{1,0:T(8,128)(2,1)S(1)} %get-tuple-element.61), channel_id=1, source_target_pairs={{0,24},{8,0},{16,8},{24,16},{2,26},{10,2},{18,10},{26,18},{4,28},{... | collective-permute-start | bytes 589832 | tf_op jit(solution)/shard_map/ppermute | solution.py:49
  160.2 3.6 %collective-permute-done.26.refs_1_ = bf16[256,384]{1,0:T(8,128)(2,1)S(1)} collective-permute-done((bf16[256,384]{1,0:T(8,128)(2,1)S(1)}, bf16[256,384]{1,0:T(8,128)(2,1)S(1)}, u32[]{:S(2)}, u32[]{:S(2)}) %collective-permute-start.26) | collective-permute-done | bytes 196640 | tf_op jit(solution)/shard_map/ppermute | solution.py:49
  163.8 1.7 collective-permute-done.27.refs_2_
  165.5 1.8 %collective-permute-done.28.refs_3_ = bf16[256,384]{1,0:T(8,128)(2,1)S(1)} collective-permute-done((bf16[256,384]{1,0:T(8,128)(2,1)S(1)}, bf16[256,384]{1,0:T(8,128)(2,1)S(1)}, u32[]{:S(2)}, u32[]{:S(2)}) %collective-permute-start.28) | collective-permute-done | bytes 196640 | tf_op jit(solution)/shard_map/ppermute | solution.py:49
  167.3 3.9 %mix.1 = bf16[384,2048]{1,0:T(8,128)(2,1)} custom-call(s32[4]{0:T(128)S(1)} %pad_add_fusion.where_ref, bf16[256,384]{1,0:T(8,128)(2,1)S(1)} %shard_map.76.refs_0_, bf16[256,384]{1,0:T(8,128)(2,1)S(1)} %collective-permute-done.26.refs_1_, bf16[256,384]{1,0:T(8,128)(2,1)S(1)} %collective-permute-done.27.refs_2_, ...), custom_call_target="tpu_custom_call" | custom-call | flops 1610612736 | bytes 4194304 | tf_op jit(solution)/shard_map/mix/pallas_call | solution.py:329
  (68 shorter events, 3.2 us)
Async XLA Ops:
  0.8 5.8 %collective-permute-start.1 = (bf16[16,2560]{1,0:T(8,128)(2,1)S(1)}, bf16[16,2560]{1,0:T(8,128)(2,1)S(1)}, u32[]{:S(2)}, u32[]{:S(2)}) collective-permute-start(bf16[16,2560]{1,0:T(8,128)(2,1)S(1)} %get-tuple-element.65), channel_id=1, source_target_pairs={{0,6},{2,0},{4,2},{6,4},{8,14},{10,8},{12,10},{14,12},{16,22},{18,... | collective-permute-start | bytes 245768 | tf_op jit(solution)/shard_map/ppermute | solution.py:49
  4.0 6.9 %collective-permute-start = (bf16[16,2560]{1,0:T(8,128)(2,1)S(1)}, bf16[16,2560]{1,0:T(8,128)(2,1)S(1)}, u32[]{:S(2)}, u32[]{:S(2)}) collective-permute-start(bf16[16,2560]{1,0:T(8,128)(2,1)S(1)} %get-tuple-element.65), channel_id=1, source_target_pairs={{0,2},{2,4},{4,6},{6,0},{8,10},{10,12},{12,14},{14,8},{16,18},{18,... | collective-permute-start | bytes 245768 | tf_op jit(solution)/shard_map/ppermute | solution.py:49
  4.0 6.9 %collective-permute-start.2 = (bf16[16,2560]{1,0:T(8,128)(2,1)S(1)}, bf16[16,2560]{1,0:T(8,128)(2,1)S(1)}, u32[]{:S(2)}, u32[]{:S(2)}) collective-permute-start(bf16[16,2560]{1,0:T(8,128)(2,1)S(1)} %get-tuple-element.65), channel_id=1, source_target_pairs={{0,4},{2,6},{4,0},{6,2},{8,12},{10,14},{12,8},{14,10},{16,20},{18,... | collective-permute-start | bytes 245768 | tf_op jit(solution)/shard_map/ppermute | solution.py:49
  11.7 7.4 %collective-permute-start.4 = (bf16[64,2560]{1,0:T(8,128)(2,1)S(1)}, bf16[64,2560]{1,0:T(8,128)(2,1)S(1)}, u32[]{:S(2)}, u32[]{:S(2)}) collective-permute-start(bf16[64,2560]{1,0:T(8,128)(2,1)S(1)} %pad_maximum_fusion.3), channel_id=1, source_target_pairs={{0,24},{8,0},{16,8},{24,16},{2,26},{10,2},{18,10},{26,18},{4,28},{... | collective-permute-start | bytes 983048 | tf_op jit(solution)/shard_map/ppermute | solution.py:49
  14.6 8.4 %collective-permute-start.3 = (bf16[64,2560]{1,0:T(8,128)(2,1)S(1)}, bf16[64,2560]{1,0:T(8,128)(2,1)S(1)}, u32[]{:S(2)}, u32[]{:S(2)}) collective-permute-start(bf16[64,2560]{1,0:T(8,128)(2,1)S(1)} %pad_maximum_fusion.3), channel_id=1, source_target_pairs={{0,8},{8,16},{16,24},{24,0},{2,10},{10,18},{18,26},{26,2},{4,12},{... | collective-permute-start | bytes 983048 | tf_op jit(solution)/shard_map/ppermute | solution.py:49
  19.2 6.6 %collective-permute-start.6 = (bf16[32,2560]{1,0:T(8,128)(2,1)S(1)}, bf16[32,2560]{1,0:T(8,128)(2,1)S(1)}, u32[]{:S(2)}, u32[]{:S(2)}) collective-permute-start(bf16[32,2560]{1,0:T(8,128)(2,1)S(1)} %slice.29), channel_id=1, source_target_pairs={{0,24},{8,0},{16,8},{24,16},{2,26},{10,2},{18,10},{26,18},{4,28},{... | collective-permute-start | bytes 491528 | tf_op jit(solution)/shard_map/ppermute | solution.py:49
  22.9 6.6 %collective-permute-start.5 = (bf16[32,2560]{1,0:T(8,128)(2,1)S(1)}, bf16[32,2560]{1,0:T(8,128)(2,1)S(1)}, u32[]{:S(2)}, u32[]{:S(2)}) collective-permute-start(bf16[32,2560]{1,0:T(8,128)(2,1)S(1)} %slice.28), channel_id=1, source_target_pairs={{0,8},{8,16},{16,24},{24,0},{2,10},{10,18},{18,26},{26,2},{4,12},{... | collective-permute-start | bytes 491528 | tf_op jit(solution)/shard_map/ppermute | solution.py:49
  23.1 34.7 %copy-start = (bf16[1,384,2048]{2,1,0:T(8,128)(2,1)S(1)}, bf16[1,384,2048]{2,1,0:T(8,128)(2,1)}, u32[]{:S(2)}) copy-start(bf16[1,384,2048]{2,1,0:T(8,128)(2,1)} %param.7) | copy-start | bytes 4718596
  29.6 4.4 %collective-permute-start.14 = (bf16[128,1536]{1,0:T(8,128)(2,1)S(1)}, bf16[128,1536]{1,0:T(8,128)(2,1)S(1)}, u32[]{:S(2)}, u32[]{:S(2)}) collective-permute-start(bf16[128,1536]{1,0:T(8,128)(2,1)S(1)} %slice.24.refs_1_), channel_id=1, source_target_pairs={{0,1},{1,0},{2,3},{3,2},{4,5},{5,4},{6,7},{7,6},{8,9},{9,8},{10,11... | collective-permute-start | bytes 1179656 | tf_op jit(solution)/shard_map/ppermute | solution.py:61
  29.7 9.4 %collective-permute-start.10 = (bf16[128,1536]{1,0:T(8,128)(2,1)S(1)}, bf16[128,1536]{1,0:T(8,128)(2,1)S(1)}, u32[]{:S(2)}, u32[]{:S(2)}) collective-permute-start(bf16[128,1536]{1,0:T(8,128)(2,1)S(1)} %slice.24.refs_1_), channel_id=1, source_target_pairs={{0,96},{32,0},{64,32},{96,64},{2,98},{34,2},{66,34},{98,66},{4,100... | collective-permute-start | bytes 1179656 | tf_op jit(solution)/shard_map/ppermute | solution.py:49
  33.8 9.0 %collective-permute-start.8 = (bf16[128,1536]{1,0:T(8,128)(2,1)S(1)}, bf16[128,1536]{1,0:T(8,128)(2,1)S(1)}, u32[]{:S(2)}, u32[]{:S(2)}) collective-permute-start(bf16[128,1536]{1,0:T(8,128)(2,1)S(1)} %slice.24.refs_1_), channel_id=1, source_target_pairs={{0,32},{32,64},{64,96},{96,0},{2,34},{34,66},{66,98},{98,2},{4,36}... | collective-permute-start | bytes 1179656 | tf_op jit(solution)/shard_map/ppermute | solution.py:49
  33.9 13.2 %collective-permute-start.7 = (bf16[128,1536]{1,0:T(8,128)(2,1)S(1)}, bf16[128,1536]{1,0:T(8,128)(2,1)S(1)}, u32[]{:S(2)}, u32[]{:S(2)}) collective-permute-start(bf16[128,1536]{1,0:T(8,128)(2,1)S(1)} %slice.23.refs_0_), channel_id=1, source_target_pairs={{0,32},{32,64},{64,96},{96,0},{2,34},{34,66},{66,98},{98,2},{4,36}... | collective-permute-start | bytes 1179656 | tf_op jit(solution)/shard_map/ppermute | solution.py:49
  33.9 13.1 %collective-permute-start.13 = (bf16[128,1536]{1,0:T(8,128)(2,1)S(1)}, bf16[128,1536]{1,0:T(8,128)(2,1)S(1)}, u32[]{:S(2)}, u32[]{:S(2)}) collective-permute-start(bf16[128,1536]{1,0:T(8,128)(2,1)S(1)} %slice.23.refs_0_), channel_id=1, source_target_pairs={{0,1},{1,0},{2,3},{3,2},{4,5},{5,4},{6,7},{7,6},{8,9},{9,8},{10,11... | collective-permute-start | bytes 1179656 | tf_op jit(solution)/shard_map/ppermute | solution.py:61
  34.0 13.0 %collective-permute-start.9 = (bf16[128,1536]{1,0:T(8,128)(2,1)S(1)}, bf16[128,1536]{1,0:T(8,128)(2,1)S(1)}, u32[]{:S(2)}, u32[]{:S(2)}) collective-permute-start(bf16[128,1536]{1,0:T(8,128)(2,1)S(1)} %slice.23.refs_0_), channel_id=1, source_target_pairs={{0,96},{32,0},{64,32},{96,64},{2,98},{34,2},{66,34},{98,66},{4,100... | collective-permute-start | bytes 1179656 | tf_op jit(solution)/shard_map/ppermute | solution.py:49
  39.1 8.4 %collective-permute-start.18 = (bf16[128,1536]{1,0:T(8,128)(2,1)S(1)}, bf16[128,1536]{1,0:T(8,128)(2,1)S(1)}, u32[]{:S(2)}, u32[]{:S(2)}) collective-permute-start(bf16[128,1536]{1,0:T(8,128)(2,1)S(1)} %collective-permute-done.10.refs_5_), channel_id=1, source_target_pairs={{0,1},{1,0},{2,3},{3,2},{4,5},{5,4},{6,7},{7,6},{8,9},{9,8},{10,11... | collective-permute-start | bytes 1179656 | tf_op jit(solution)/shard_map/ppermute | solution.py:61
  42.8 7.8 %collective-permute-start.12 = (bf16[128,1536]{1,0:T(8,128)(2,1)S(1)}, bf16[128,1536]{1,0:T(8,128)(2,1)S(1)}, u32[]{:S(2)}, u32[]{:S(2)}) collective-permute-start(bf16[128,1536]{1,0:T(8,128)(2,1)S(1)} %collective-permute-done.10.refs_5_), channel_id=1, source_target_pairs={{0,96},{32,0},{64,32},{96,64},{2,98},{34,2},{66,34},{98,66},{4,100... | collective-permute-start | bytes 1179656 | tf_op jit(solution)/shard_map/ppermute | solution.py:49
  47.0 9.0 %collective-permute-start.11 = (bf16[128,1536]{1,0:T(8,128)(2,1)S(1)}, bf16[128,1536]{1,0:T(8,128)(2,1)S(1)}, u32[]{:S(2)}, u32[]{:S(2)}) collective-permute-start(bf16[128,1536]{1,0:T(8,128)(2,1)S(1)} %collective-permute-done.7.refs_2_), channel_id=1, source_target_pairs={{0,32},{32,64},{64,96},{96,0},{2,34},{34,66},{66,98},{98,2},{4,36}... | collective-permute-start | bytes 1179656 | tf_op jit(solution)/shard_map/ppermute | solution.py:49
  47.0 9.0 %collective-permute-start.15 = (bf16[128,1536]{1,0:T(8,128)(2,1)S(1)}, bf16[128,1536]{1,0:T(8,128)(2,1)S(1)}, u32[]{:S(2)}, u32[]{:S(2)}) collective-permute-start(bf16[128,1536]{1,0:T(8,128)(2,1)S(1)} %collective-permute-done.7.refs_2_), channel_id=1, source_target_pairs={{0,1},{1,0},{2,3},{3,2},{4,5},{5,4},{6,7},{7,6},{8,9},{9,8},{10,11... | collective-permute-start | bytes 1179656 | tf_op jit(solution)/shard_map/ppermute | solution.py:61
  47.1 9.0 %collective-permute-start.16 = (bf16[128,1536]{1,0:T(8,128)(2,1)S(1)}, bf16[128,1536]{1,0:T(8,128)(2,1)S(1)}, u32[]{:S(2)}, u32[]{:S(2)}) collective-permute-start(bf16[128,1536]{1,0:T(8,128)(2,1)S(1)} %collective-permute-done.8.refs_3_), channel_id=1, source_target_pairs={{0,1},{1,0},{2,3},{3,2},{4,5},{5,4},{6,7},{7,6},{8,9},{9,8},{10,11... | collective-permute-start | bytes 1179656 | tf_op jit(solution)/shard_map/ppermute | solution.py:61
  47.6 8.5 %collective-permute-start.17 = (bf16[128,1536]{1,0:T(8,128)(2,1)S(1)}, bf16[128,1536]{1,0:T(8,128)(2,1)S(1)}, u32[]{:S(2)}, u32[]{:S(2)}) collective-permute-start(bf16[128,1536]{1,0:T(8,128)(2,1)S(1)} %collective-permute-done.9.refs_4_), channel_id=1, source_target_pairs={{0,1},{1,0},{2,3},{3,2},{4,5},{5,4},{6,7},{7,6},{8,9},{9,8},{10,11... | collective-permute-start | bytes 1179656 | tf_op jit(solution)/shard_map/ppermute | solution.py:61
  50.6 5.4 %collective-permute-start.20 = (bf16[128,1536]{1,0:T(8,128)(2,1)S(1)}, bf16[128,1536]{1,0:T(8,128)(2,1)S(1)}, u32[]{:S(2)}, u32[]{:S(2)}) collective-permute-start(bf16[128,1536]{1,0:T(8,128)(2,1)S(1)} %collective-permute-done.12.refs_7_), channel_id=1, source_target_pairs={{0,1},{1,0},{2,3},{3,2},{4,5},{5,4},{6,7},{7,6},{8,9},{9,8},{10,11... | collective-permute-start | bytes 1179656 | tf_op jit(solution)/shard_map/ppermute | solution.py:61
  56.0 1.7 %collective-permute-start.19 = (bf16[128,1536]{1,0:T(8,128)(2,1)S(1)}, bf16[128,1536]{1,0:T(8,128)(2,1)S(1)}, u32[]{:S(2)}, u32[]{:S(2)}) collective-permute-start(bf16[128,1536]{1,0:T(8,128)(2,1)S(1)} %collective-permute-done.11.refs_6_), channel_id=1, source_target_pairs={{0,1},{1,0},{2,3},{3,2},{4,5},{5,4},{6,7},{7,6},{8,9},{9,8},{10,11... | collective-permute-start | bytes 1179656 | tf_op jit(solution)/shard_map/ppermute | solution.py:61
  62.6 15.1 %all-to-all-start = ((bf16[4,384,384]{2,1,0:T(8,128)(2,1)}), bf16[4,384,384]{2,1,0:T(8,128)(2,1)S(1)}, u32[]{:S(2)}, u32[]{:S(2)}) async-start(bf16[4,384,384]{2,1,0:T(8,128)(2,1)} %project.1), calls=%async_computation | async-start | bytes 2359296 | tf_op jit(solution)/shard_map/all_to_all | solution.py:389
  77.8 20.7 %collective-permute-start.21 = (bf16[4,128,384]{2,1,0:T(8,128)(2,1)S(1)}, bf16[4,128,384]{2,1,0:T(8,128)(2,1)S(1)}, u32[]{:S(2)}, u32[]{:S(2)}) collective-permute-start(bf16[4,128,384]{2,1,0:T(8,128)(2,1)S(1)} %slice.27), channel_id=1, source_target_pairs={{0,32},{32,0},{64,96},{96,64},{2,34},{34,2},{66,98},{98,66},{4,36}... | collective-permute-start | bytes 1179656 | tf_op jit(solution)/shard_map/ppermute | solution.py:57
  77.9 39.4 %collective-permute-start.23 = (bf16[256,1024]{1,0:T(8,128)(2,1)S(1)}, bf16[256,1024]{1,0:T(8,128)(2,1)S(1)}, u32[]{:S(2)}, u32[]{:S(2)}) collective-permute-start(bf16[256,1024]{1,0:T(8,128)(2,1)S(1)} %pad_maximum_fusion.2), channel_id=1, source_target_pairs={{0,32},{32,0},{64,96},{96,64},{2,34},{34,2},{66,98},{98,66},{4,36}... | collective-permute-start | bytes 1572872 | tf_op jit(solution)/shard_map/ppermute | solution.py:57
  98.6 18.7 %collective-permute-start.22 = (bf16[8,128,384]{2,1,0:T(8,128)(2,1)S(1)}, bf16[8,128,384]{2,1,0:T(8,128)(2,1)S(1)}, u32[]{:S(2)}, u32[]{:S(2)}) collective-permute-start(bf16[8,128,384]{2,1,0:T(8,128)(2,1)S(1)} %pad_maximum_fusion), channel_id=1, source_target_pairs={{0,96},{32,64},{64,32},{96,0},{2,98},{34,66},{66,34},{98,2},{4,100... | collective-permute-start | bytes 2359304 | tf_op jit(solution)/shard_map/ppermute | solution.py:57
  117.3 39.0 %collective-permute-start.25 = (bf16[512,1024]{1,0:T(8,128)(2,1)S(1)}, bf16[512,1024]{1,0:T(8,128)(2,1)S(1)}, u32[]{:S(2)}, u32[]{:S(2)}) collective-permute-start(bf16[512,1024]{1,0:T(8,128)(2,1)S(1)} %constant_dynamic-update-slice_fusion.5.refs_4_), channel_id=1, source_target_pairs={{0,96},{32,64},{64,32},{96,0},{2,98},{34,66},{66,34},{98,2},{4,100... | collective-permute-start | bytes 3145736 | tf_op jit(solution)/shard_map/ppermute | solution.py:57
  120.6 26.9 %collective-permute-start.24 = (bf16[512,1024]{1,0:T(8,128)(2,1)S(1)}, bf16[512,1024]{1,0:T(8,128)(2,1)S(1)}, u32[]{:S(2)}, u32[]{:S(2)}) collective-permute-start(bf16[512,1024]{1,0:T(8,128)(2,1)S(1)} %constant_dynamic-update-slice_fusion.5.refs_4_), channel_id=1, source_target_pairs={{0,1},{1,0},{2,3},{3,2},{4,5},{5,4},{6,7},{7,6},{8,9},{9,8},{10,11... | collective-permute-start | bytes 3145736 | tf_op jit(solution)/shard_map/ppermute | solution.py:61
  156.3 11.0 %collective-permute-start.29 = (bf16[512,1024]{1,0:T(8,128)(2,1)S(1)}, bf16[512,1024]{1,0:T(8,128)(2,1)S(1)}, u32[]{:S(2)}, u32[]{:S(2)}) collective-permute-start(bf16[512,1024]{1,0:T(8,128)(2,1)S(1)} %collective-permute-done.25.refs_5_), channel_id=1, source_target_pairs={{0,1},{1,0},{2,3},{3,2},{4,5},{5,4},{6,7},{7,6},{8,9},{9,8},{10,11... | collective-permute-start | bytes 3145736 | tf_op jit(solution)/shard_map/ppermute | solution.py:61
  156.9 6.9 %collective-permute-start.26 = (bf16[256,384]{1,0:T(8,128)(2,1)S(1)}, bf16[256,384]{1,0:T(8,128)(2,1)S(1)}, u32[]{:S(2)}, u32[]{:S(2)}) collective-permute-start(bf16[256,384]{1,0:T(8,128)(2,1)S(1)} %get-tuple-element.60), channel_id=1, source_target_pairs={{0,8},{8,16},{16,24},{24,0},{2,10},{10,18},{18,26},{26,2},{4,12},{... | collective-permute-start | bytes 589832 | tf_op jit(solution)/shard_map/ppermute | solution.py:49
  157.5 8.0 %collective-permute-start.27 = (bf16[256,384]{1,0:T(8,128)(2,1)S(1)}, bf16[256,384]{1,0:T(8,128)(2,1)S(1)}, u32[]{:S(2)}, u32[]{:S(2)}) collective-permute-start(bf16[256,384]{1,0:T(8,128)(2,1)S(1)} %get-tuple-element.61), channel_id=1, source_target_pairs={{0,24},{8,0},{16,8},{24,16},{2,26},{10,2},{18,10},{26,18},{4,28},{... | collective-permute-start | bytes 589832 | tf_op jit(solution)/shard_map/ppermute | solution.py:49
  160.2 7.2 %collective-permute-start.28 = (bf16[256,384]{1,0:T(8,128)(2,1)S(1)}, bf16[256,384]{1,0:T(8,128)(2,1)S(1)}, u32[]{:S(2)}, u32[]{:S(2)}) collective-permute-start(bf16[256,384]{1,0:T(8,128)(2,1)S(1)} %get-tuple-element.62), channel_id=1, source_target_pairs={{0,16},{8,24},{16,0},{24,8},{2,18},{10,26},{18,2},{26,10},{4,20},{... | collective-permute-start | bytes 589832 | tf_op jit(solution)/shard_map/ppermute | solution.py:49
  (2 other events, 69.3 us)
where the time goes:
time: 172 us; the launch traced here: 171 us
  Pallas kernels  81.6 us (47%)
  waiting for transfers between devices  53.5 us (31%)
  starting transfers between devices  33.2 us (19%)
  other arithmetic  2.27 us (1%)
    pallas_call x4, Pallas kernels, attend(): pl.pallas_call(kern, grid_spec=pltpu.PrefetchScalarGridSpec(num_scalar_pr...  72.8 us
    ppermute x16, waiting for transfers between devices, shift(): return lax.ppermute(array, AXES, shift_pairs(axis_of_core, step))  40.5 us
    ppermute x16, starting transfers between devices, shift(): return lax.ppermute(array, AXES, shift_pairs(axis_of_core, step))  22.8 us
    all_to_all x1, waiting for transfers between devices, per_device(): lax.all_to_all(qkv, AXES, split_axis=0, concat_axis=0, tiled=True, axis_i...  11.3 us
    ppermute x4, starting transfers between devices, pair(): return lax.ppermute(array, AXES, pairs)  5.47 us
    pallas_call x1, Pallas kernels, project(): pl.pallas_call(kern, in_specs=[pl.BlockSpec(memory_space=pltpu.SMEM)] + [...  4.89 us
    pallas_call x1, Pallas kernels, mix(): pl.pallas_call(kern, in_specs=[pl.BlockSpec(memory_space=pltpu.SMEM), *[p...  3.9 us
    all_to_all x1, starting transfers between devices, per_device(): lax.all_to_all(qkv, AXES, split_axis=0, concat_axis=0, tiled=True, axis_i...  3.53 us
  transfers between devices with their start and end apart: 31, of which 14 were waited for; matrix products, arithmetic and copies ran while one was open for 0% of the time, Pallas kernels for 43%

commit v1 on v0

--- a/solution.py
+++ b/solution.py
@@ -397,23 +397,24 @@
     away = jnp.stack(ring_order(here)[1:])
     kv_own = qkv[:, GROUP * HEAD :, :]
     kv_near = pair(kv_own, OUTER, False)
+    kv_next = pair(kv_own, OUTER, True)
     out_near = pair(out_own, OUTER, False)
     sums = attend(every, q_row, k_row, qkv, [qkv], None, False)
-    sums, kv_own, kv_near = lax.optimization_barrier((sums, kv_own, kv_near))
-    kv_other = pair(jnp.concatenate([kv_own, kv_near], axis=0), OUTER, True)
+    sums, kv_near, kv_next = lax.optimization_barrier((sums, kv_near, kv_next))
+    kv_far = pair(kv_near, OUTER, True)
     sums = attend(every, q_row, k_row, qkv, [kv_near], sums, False)
-    sums, kv_other, out_near = lax.optimization_barrier((sums, kv_other, out_near))
+    sums, kv_next, kv_far, out_near = lax.optimization_barrier((sums, kv_next, kv_far, out_near))
     out_half = jnp.concatenate([out_own, out_near], axis=0)
     out_other = pair(out_half, OUTER, True)
     out_half_theirs = swap(out_half)
-    behind, ahead, across = attend(away, q_row, k_row, qkv, [kv_other], sums, True)
-    sums, kv_other, behind, ahead, across, out_half_theirs = lax.optimization_barrier(
-        (sums, kv_other, behind, ahead, across, out_half_theirs)
+    behind, ahead, across = attend(away, q_row, k_row, qkv, [kv_next, kv_far], sums, True)
+    sums, kv_next, kv_far, behind, ahead, across, out_half_theirs = lax.optimization_barrier(
+        (sums, kv_next, kv_far, behind, ahead, across, out_half_theirs)
     )
     across = shift(across, INNER, 2)
     ahead = shift(ahead, INNER, 1)
     behind = shift(behind, INNER, -1)
-    (own,) = attend(here.reshape(1), q_row, k_row, qkv, [kv_other], sums, True)
+    (own,) = attend(here.reshape(1), q_row, k_row, qkv, [kv_next, kv_far], sums, True)
     own, out_other = lax.optimization_barrier((own, out_other))
     out_other_theirs = swap(out_other)
     return mix(

time: 172 us -> 172 us (level)
    ppermute x4 -> x5, starting transfers between devices: 5.47 us -> 5.58 us  [pair(): return lax.ppermute(array, AXES, pairs)]
  transfers between devices with their start and end apart: 31 -> 32, of which waited for: 14 -> 14; matrix products, arithmetic and copies ran while one was open for 0% -> 0% of each run, Pallas kernels for 43% -> 42%
where the time goes in v1:
time: 172 us; the launch traced here: 171 us
  Pallas kernels  81.6 us (47%)
  waiting for transfers between devices  53.5 us (31%)
  starting transfers between devices  33.5 us (19%)
  other arithmetic  2.17 us (1%)
    pallas_call x4, Pallas kernels, attend(): pl.pallas_call(kern, grid_spec=pltpu.PrefetchScalarGridSpec(num_scalar_pr...  72.8 us
    ppermute x16, waiting for transfers between devices, shift(): return lax.ppermute(array, AXES, shift_pairs(axis_of_core, step))  40.5 us
    ppermute x16, starting transfers between devices, shift(): return lax.ppermute(array, AXES, shift_pairs(axis_of_core, step))  22.8 us
    all_to_all x1, waiting for transfers between devices, per_device(): lax.all_to_all(qkv, AXES, split_axis=0, concat_axis=0, tiled=True, axis_i...  11.3 us
    ppermute x5, starting transfers between devices, pair(): return lax.ppermute(array, AXES, pairs)  5.58 us
    pallas_call x1, Pallas kernels, project(): pl.pallas_call(kern, in_specs=[pl.BlockSpec(memory_space=pltpu.SMEM)] + [...  4.89 us
    pallas_call x1, Pallas kernels, mix(): pl.pallas_call(kern, in_specs=[pl.BlockSpec(memory_space=pltpu.SMEM), *[p...  3.9 us
    all_to_all x1, starting transfers between devices, per_device(): lax.all_to_all(qkv, AXES, split_axis=0, concat_axis=0, tiled=True, axis_i...  3.53 us
  transfers between devices with their start and end apart: 32, of which 14 were waited for; matrix products, arithmetic and copies ran while one was open for 0% of the time, Pallas kernels for 42%

profile of v1, /device:TPU:0, one launch (start us, length us, event | category | flops | bytes accessed | tf_op | source)
XLA Modules:
  0.0 171.5 jit_solution(1923217385307346325)
XLA Ops:
  0.0 0.8 pad_maximum_fusion.4
  0.8 3.2 %collective-permute-start.1 = (bf16[16,2560]{1,0:T(8,128)(2,1)S(1)}, bf16[16,2560]{1,0:T(8,128)(2,1)S(1)}, u32[]{:S(2)}, u32[]{:S(2)}) collective-permute-start(bf16[16,2560]{1,0:T(8,128)(2,1)S(1)} %get-tuple-element.69), channel_id=1, source_target_pairs={{0,6},{2,0},{4,2},{6,4},{8,14},{10,8},{12,10},{14,12},{16,22},{18,... | collective-permute-start | bytes 245768 | tf_op jit(solution)/shard_map/ppermute | solution.py:49
  4.0 2.2 %collective-permute-start.2 = (bf16[16,2560]{1,0:T(8,128)(2,1)S(1)}, bf16[16,2560]{1,0:T(8,128)(2,1)S(1)}, u32[]{:S(2)}, u32[]{:S(2)}) collective-permute-start(bf16[16,2560]{1,0:T(8,128)(2,1)S(1)} %get-tuple-element.69), channel_id=1, source_target_pairs={{0,4},{2,6},{4,0},{6,2},{8,12},{10,14},{12,8},{14,10},{16,20},{18,... | collective-permute-start | bytes 245768 | tf_op jit(solution)/shard_map/ppermute | solution.py:49
  6.6 4.3 %collective-permute-done = bf16[16,2560]{1,0:T(8,128)(2,1)S(1)} collective-permute-done((bf16[16,2560]{1,0:T(8,128)(2,1)S(1)}, bf16[16,2560]{1,0:T(8,128)(2,1)S(1)}, u32[]{:S(2)}, u32[]{:S(2)}) %collective-permute-start) | collective-permute-done | bytes 81952 | tf_op jit(solution)/shard_map/ppermute | solution.py:49
  10.9 0.8 pad_maximum_fusion.2
  11.7 2.8 %collective-permute-start.4 = (bf16[64,2560]{1,0:T(8,128)(2,1)S(1)}, bf16[64,2560]{1,0:T(8,128)(2,1)S(1)}, u32[]{:S(2)}, u32[]{:S(2)}) collective-permute-start(bf16[64,2560]{1,0:T(8,128)(2,1)S(1)} %pad_maximum_fusion.2), channel_id=1, source_target_pairs={{0,24},{8,0},{16,8},{24,16},{2,26},{10,2},{18,10},{26,18},{4,28},{... | collective-permute-start | bytes 983048 | tf_op jit(solution)/shard_map/ppermute | solution.py:49
  14.6 4.5 %collective-permute-done.4 = bf16[64,2560]{1,0:T(8,128)(2,1)S(1)} collective-permute-done((bf16[64,2560]{1,0:T(8,128)(2,1)S(1)}, bf16[64,2560]{1,0:T(8,128)(2,1)S(1)}, u32[]{:S(2)}, u32[]{:S(2)}) %collective-permute-start.4) | collective-permute-done | bytes 327712 | tf_op jit(solution)/shard_map/ppermute | solution.py:49
  19.2 3.8 %collective-permute-start.6 = (bf16[32,2560]{1,0:T(8,128)(2,1)S(1)}, bf16[32,2560]{1,0:T(8,128)(2,1)S(1)}, u32[]{:S(2)}, u32[]{:S(2)}) collective-permute-start(bf16[32,2560]{1,0:T(8,128)(2,1)S(1)} %slice.29), channel_id=1, source_target_pairs={{0,24},{8,0},{16,8},{24,16},{2,26},{10,2},{18,10},{26,18},{4,28},{... | collective-permute-start | bytes 491528 | tf_op jit(solution)/shard_map/ppermute | solution.py:49
  23.1 2.7 %collective-permute-done.6 = bf16[32,2560]{1,0:T(8,128)(2,1)S(1)} collective-permute-done((bf16[32,2560]{1,0:T(8,128)(2,1)S(1)}, bf16[32,2560]{1,0:T(8,128)(2,1)S(1)}, u32[]{:S(2)}, u32[]{:S(2)}) %collective-permute-start.6) | collective-permute-done | bytes 163872 | tf_op jit(solution)/shard_map/ppermute | solution.py:49
  25.8 3.8 %collective-permute-done.5 = bf16[32,2560]{1,0:T(8,128)(2,1)S(1)} collective-permute-done((bf16[32,2560]{1,0:T(8,128)(2,1)S(1)}, bf16[32,2560]{1,0:T(8,128)(2,1)S(1)}, u32[]{:S(2)}, u32[]{:S(2)}) %collective-permute-start.5) | collective-permute-done | bytes 163872 | tf_op jit(solution)/shard_map/ppermute | solution.py:49
  29.7 4.1 %collective-permute-start.10 = (bf16[128,1536]{1,0:T(8,128)(2,1)S(1)}, bf16[128,1536]{1,0:T(8,128)(2,1)S(1)}, u32[]{:S(2)}, u32[]{:S(2)}) collective-permute-start(bf16[128,1536]{1,0:T(8,128)(2,1)S(1)} %slice.24.refs_1_), channel_id=1, source_target_pairs={{0,96},{32,0},{64,32},{96,64},{2,98},{34,2},{66,34},{98,66},{4,100... | collective-permute-start | bytes 1179656 | tf_op jit(solution)/shard_map/ppermute | solution.py:49
  34.0 3.3 %collective-permute-start.9 = (bf16[128,1536]{1,0:T(8,128)(2,1)S(1)}, bf16[128,1536]{1,0:T(8,128)(2,1)S(1)}, u32[]{:S(2)}, u32[]{:S(2)}) collective-permute-start(bf16[128,1536]{1,0:T(8,128)(2,1)S(1)} %slice.23.refs_0_), channel_id=1, source_target_pairs={{0,96},{32,0},{64,32},{96,64},{2,98},{34,2},{66,34},{98,66},{4,100... | collective-permute-start | bytes 1179656 | tf_op jit(solution)/shard_map/ppermute | solution.py:49
  37.3 1.8 %collective-permute-done.10.refs_5_ = bf16[128,1536]{1,0:T(8,128)(2,1)S(1)} collective-permute-done((bf16[128,1536]{1,0:T(8,128)(2,1)S(1)}, bf16[128,1536]{1,0:T(8,128)(2,1)S(1)}, u32[]{:S(2)}, u32[]{:S(2)}) %collective-permute-start.10) | collective-permute-done | bytes 393248 | tf_op jit(solution)/shard_map/ppermute | solution.py:49
  39.1 3.7 %collective-permute-done.8.refs_3_ = bf16[128,1536]{1,0:T(8,128)(2,1)S(1)} collective-permute-done((bf16[128,1536]{1,0:T(8,128)(2,1)S(1)}, bf16[128,1536]{1,0:T(8,128)(2,1)S(1)}, u32[]{:S(2)}, u32[]{:S(2)}) %collective-permute-start.8) | collective-permute-done | bytes 393248 | tf_op jit(solution)/shard_map/ppermute | solution.py:49
  42.8 4.2 %collective-permute-done.7.refs_2_ = bf16[128,1536]{1,0:T(8,128)(2,1)S(1)} collective-permute-done((bf16[128,1536]{1,0:T(8,128)(2,1)S(1)}, bf16[128,1536]{1,0:T(8,128)(2,1)S(1)}, u32[]{:S(2)}, u32[]{:S(2)}) %collective-permute-start.7) | collective-permute-done | bytes 393248 | tf_op jit(solution)/shard_map/ppermute | solution.py:49
  47.6 2.9 %collective-permute-done.12.refs_7_ = bf16[128,1536]{1,0:T(8,128)(2,1)S(1)} collective-permute-done((bf16[128,1536]{1,0:T(8,128)(2,1)S(1)}, bf16[128,1536]{1,0:T(8,128)(2,1)S(1)}, u32[]{:S(2)}, u32[]{:S(2)}) %collective-permute-start.12) | collective-permute-done | bytes 393248 | tf_op jit(solution)/shard_map/ppermute | solution.py:49
  50.6 5.4 %collective-permute-done.11.refs_6_ = bf16[128,1536]{1,0:T(8,128)(2,1)S(1)} collective-permute-done((bf16[128,1536]{1,0:T(8,128)(2,1)S(1)}, bf16[128,1536]{1,0:T(8,128)(2,1)S(1)}, u32[]{:S(2)}, u32[]{:S(2)}) %collective-permute-start.11) | collective-permute-done | bytes 393248 | tf_op jit(solution)/shard_map/ppermute | solution.py:49
  56.0 1.7 collective-permute-done.19.refs_14_
  57.8 4.9 %project.1 = bf16[4,384,384]{2,1,0:T(8,128)(2,1)} custom-call(s32[4]{0:T(128)S(1)} %pad_add_fusion.where_ref, bf16[384,2048]{1,0:T(8,128)(2,1)S(1)} %bitcast.13, bf16[128,1536]{1,0:T(8,128)(2,1)S(1)} %slice.23.refs_0_, bf16[128,1536]{1,0:T(8,128)(2,1)S(1)} %slice.24.refs_1_, bf16[128,1536]{1,0:T(8,128)(2,1)S(1)} %collective-permute-done.7.refs_2_, ...), custom_call_target="tpu_custom_call" | custom-call | flops 2415919104 | bytes 6291456 | tf_op jit(solution)/shard_map/project/pallas_call | solution.py:150
  62.6 3.5 %all-to-all-start = ((bf16[4,384,384]{2,1,0:T(8,128)(2,1)}), bf16[4,384,384]{2,1,0:T(8,128)(2,1)S(1)}, u32[]{:S(2)}, u32[]{:S(2)}) async-start(bf16[4,384,384]{2,1,0:T(8,128)(2,1)} %project.1), calls=%async_computation | async-start | bytes 2359296 | tf_op jit(solution)/shard_map/all_to_all | solution.py:389
  66.4 11.3 %all-to-all-done.q_ref.refs_0_ = bf16[4,384,384]{2,1,0:T(8,128)(2,1)S(1)} async-done(((bf16[4,384,384]{2,1,0:T(8,128)(2,1)}), bf16[4,384,384]{2,1,0:T(8,128)(2,1)S(1)}, u32[]{:S(2)}, u32[]{:S(2)}) %all-to-all-start) | async-done | bytes 1179680 | tf_op jit(solution)/shard_map/all_to_all | solution.py:389
  78.0 2.0 %collective-permute-start.24 = (bf16[256,1024]{1,0:T(8,128)(2,1)S(1)}, bf16[256,1024]{1,0:T(8,128)(2,1)S(1)}, u32[]{:S(2)}, u32[]{:S(2)}) collective-permute-start(bf16[256,1024]{1,0:T(8,128)(2,1)S(1)} %pad_maximum_fusion.1), channel_id=1, source_target_pairs={{0,32},{32,0},{64,96},{96,64},{2,34},{34,2},{66,98},{98,66},{4,36}... | collective-permute-start | bytes 1572872 | tf_op jit(solution)/shard_map/ppermute | solution.py:57
  80.0 18.6 %shard_map.73 = (f32[4,80,1536]{2,1,0:T(8,128)S(1)}, f32[4,8,1536]{2,1,0:T(8,128)S(1)}) custom-call(s32[4]{0:T(128)S(1)} %iota.22.place_ref, f32[1,64]{1,0:T(1,128)S(1)} %bitcast.15, f32[1,64]{1,0:T(1,128)S(1)} %bitcast.20, bf16[4,384,384]{2,1,0:T(8,128)(2,1)S(1)} %all-to-all-done.q_ref.refs_0_, bf16[4,384,384]{2,1,0:T(8,128)(2,1)S(1)} %all-to-all-done.q_ref.refs_0_), custom_call_target="tpu_custom_call" | custom-call | flops 19327352832 | bytes 393216 | tf_op jit(solution)/shard_map/pallas_call | solution.py:275
  98.6 3.2 %collective-permute-start.23 = (bf16[4,128,384]{2,1,0:T(8,128)(2,1)S(1)}, bf16[4,128,384]{2,1,0:T(8,128)(2,1)S(1)}, u32[]{:S(2)}, u32[]{:S(2)}) collective-permute-start(bf16[4,128,384]{2,1,0:T(8,128)(2,1)S(1)} %collective-permute-done.21.refs_0_), channel_id=1, source_target_pairs={{0,96},{32,64},{64,32},{96,0},{2,98},{34,66},{66,34},{98,2},{4,100... | collective-permute-start | bytes 1179656 | tf_op jit(solution)/shard_map/ppermute | solution.py:57
  101.8 18.6 %shard_map.74 = (f32[4,80,1536]{2,1,0:T(8,128)S(1)}, f32[4,8,1536]{2,1,0:T(8,128)S(1)}) custom-call(s32[4]{0:T(128)S(1)} %iota.21.place_ref, f32[1,64]{1,0:T(1,128)S(1)} %bitcast.16, f32[1,64]{1,0:T(1,128)S(1)} %bitcast.21, bf16[4,384,384]{2,1,0:T(8,128)(2,1)S(1)} %all-to-all-done.q_ref.refs_0_, bf16[4,128,384]{2,1,0:T(8,128)(2,1)S(1)} %collective-permute-done.21.refs_0_, ...), custom_call_target="tpu_custom_call" | custom-call | flops 19327352832 | bytes 393216 | tf_op jit(solution)/shard_map/pallas_call | solution.py:275
  120.9 26.9 %shard_map.75 = (bf16[256,384]{1,0:T(8,128)(2,1)S(1)}, bf16[256,384]{1,0:T(8,128)(2,1)S(1)}, bf16[256,384]{1,0:T(8,128)(2,1)S(1)}) custom-call(s32[3]{0:T(128)S(1)} %pad_add_fusion.1.place_ref, f32[1,64]{1,0:T(1,128)S(1)} %bitcast.17, f32[1,64]{1,0:T(1,128)S(1)} %bitcast.22, bf16[4,384,384]{2,1,0:T(8,128)(2,1)S(1)} %all-to-all-done.q_ref.refs_0_, ...), custom_call_target="tpu_custom_call" | custom-call | flops 28991029248 | bytes 786432 | tf_op jit(solution)/shard_map/pallas_call | solution.py:275
  147.8 8.8 %shard_map.76.refs_0_ = bf16[256,384]{1,0:T(8,128)(2,1)S(1)} custom-call(s32[1]{0:T(128)} %bitcast.5.place_ref, f32[1,64]{1,0:T(1,128)S(1)} %bitcast.18, f32[1,64]{1,0:T(1,128)S(1)} %bitcast.23, bf16[4,384,384]{2,1,0:T(8,128)(2,1)S(1)} %all-to-all-done.q_ref.refs_0_, bf16[4,128,384]{2,1,0:T(8,128)(2,1)S(1)} %collective-permute-done.22.refs_0_, ...), custom_call_target="tpu_custom_call" | custom-call | flops 9663676416 | bytes 786432 | tf_op jit(solution)/shard_map/pallas_call | solution.py:275
  157.7 2.7 %collective-permute-start.28 = (bf16[256,384]{1,0:T(8,128)(2,1)S(1)}, bf16[256,384]{1,0:T(8,128)(2,1)S(1)}, u32[]{:S(2)}, u32[]{:S(2)}) collective-permute-start(bf16[256,384]{1,0:T(8,128)(2,1)S(1)} %get-tuple-element.65), channel_id=1, source_target_pairs={{0,24},{8,0},{16,8},{24,16},{2,26},{10,2},{18,10},{26,18},{4,28},{... | collective-permute-start | bytes 589832 | tf_op jit(solution)/shard_map/ppermute | solution.py:49
  160.4 3.6 %collective-permute-done.27.refs_1_ = bf16[256,384]{1,0:T(8,128)(2,1)S(1)} collective-permute-done((bf16[256,384]{1,0:T(8,128)(2,1)S(1)}, bf16[256,384]{1,0:T(8,128)(2,1)S(1)}, u32[]{:S(2)}, u32[]{:S(2)}) %collective-permute-start.27) | collective-permute-done | bytes 196640 | tf_op jit(solution)/shard_map/ppermute | solution.py:49
  164.1 1.7 collective-permute-done.28.refs_2_
  165.7 1.8 %collective-permute-done.29.refs_3_ = bf16[256,384]{1,0:T(8,128)(2,1)S(1)} collective-permute-done((bf16[256,384]{1,0:T(8,128)(2,1)S(1)}, bf16[256,384]{1,0:T(8,128)(2,1)S(1)}, u32[]{:S(2)}, u32[]{:S(2)}) %collective-permute-start.29) | collective-permute-done | bytes 196640 | tf_op jit(solution)/shard_map/ppermute | solution.py:49
  167.6 3.9 %mix.1 = bf16[384,2048]{1,0:T(8,128)(2,1)} custom-call(s32[4]{0:T(128)S(1)} %pad_add_fusion.where_ref, bf16[256,384]{1,0:T(8,128)(2,1)S(1)} %shard_map.76.refs_0_, bf16[256,384]{1,0:T(8,128)(2,1)S(1)} %collective-permute-done.27.refs_1_, bf16[256,384]{1,0:T(8,128)(2,1)S(1)} %collective-permute-done.28.refs_2_, ...), custom_call_target="tpu_custom_call" | custom-call | flops 1610612736 | bytes 4194304 | tf_op jit(solution)/shard_map/mix/pallas_call | solution.py:329
  (69 shorter events, 3.5 us)
Async XLA Ops:
  0.8 5.8 %collective-permute-start.1 = (bf16[16,2560]{1,0:T(8,128)(2,1)S(1)}, bf16[16,2560]{1,0:T(8,128)(2,1)S(1)}, u32[]{:S(2)}, u32[]{:S(2)}) collective-permute-start(bf16[16,2560]{1,0:T(8,128)(2,1)S(1)} %get-tuple-element.69), channel_id=1, source_target_pairs={{0,6},{2,0},{4,2},{6,4},{8,14},{10,8},{12,10},{14,12},{16,22},{18,... | collective-permute-start | bytes 245768 | tf_op jit(solution)/shard_map/ppermute | solution.py:49
  4.0 6.9 %collective-permute-start = (bf16[16,2560]{1,0:T(8,128)(2,1)S(1)}, bf16[16,2560]{1,0:T(8,128)(2,1)S(1)}, u32[]{:S(2)}, u32[]{:S(2)}) collective-permute-start(bf16[16,2560]{1,0:T(8,128)(2,1)S(1)} %get-tuple-element.69), channel_id=1, source_target_pairs={{0,2},{2,4},{4,6},{6,0},{8,10},{10,12},{12,14},{14,8},{16,18},{18,... | collective-permute-start | bytes 245768 | tf_op jit(solution)/shard_map/ppermute | solution.py:49
  4.0 6.9 %collective-permute-start.2 = (bf16[16,2560]{1,0:T(8,128)(2,1)S(1)}, bf16[16,2560]{1,0:T(8,128)(2,1)S(1)}, u32[]{:S(2)}, u32[]{:S(2)}) collective-permute-start(bf16[16,2560]{1,0:T(8,128)(2,1)S(1)} %get-tuple-element.69), channel_id=1, source_target_pairs={{0,4},{2,6},{4,0},{6,2},{8,12},{10,14},{12,8},{14,10},{16,20},{18,... | collective-permute-start | bytes 245768 | tf_op jit(solution)/shard_map/ppermute | solution.py:49
  11.7 7.4 %collective-permute-start.4 = (bf16[64,2560]{1,0:T(8,128)(2,1)S(1)}, bf16[64,2560]{1,0:T(8,128)(2,1)S(1)}, u32[]{:S(2)}, u32[]{:S(2)}) collective-permute-start(bf16[64,2560]{1,0:T(8,128)(2,1)S(1)} %pad_maximum_fusion.2), channel_id=1, source_target_pairs={{0,24},{8,0},{16,8},{24,16},{2,26},{10,2},{18,10},{26,18},{4,28},{... | collective-permute-start | bytes 983048 | tf_op jit(solution)/shard_map/ppermute | solution.py:49
  14.6 8.4 %collective-permute-start.3 = (bf16[64,2560]{1,0:T(8,128)(2,1)S(1)}, bf16[64,2560]{1,0:T(8,128)(2,1)S(1)}, u32[]{:S(2)}, u32[]{:S(2)}) collective-permute-start(bf16[64,2560]{1,0:T(8,128)(2,1)S(1)} %pad_maximum_fusion.2), channel_id=1, source_target_pairs={{0,8},{8,16},{16,24},{24,0},{2,10},{10,18},{18,26},{26,2},{4,12},{... | collective-permute-start | bytes 983048 | tf_op jit(solution)/shard_map/ppermute | solution.py:49
  19.2 6.6 %collective-permute-start.6 = (bf16[32,2560]{1,0:T(8,128)(2,1)S(1)}, bf16[32,2560]{1,0:T(8,128)(2,1)S(1)}, u32[]{:S(2)}, u32[]{:S(2)}) collective-permute-start(bf16[32,2560]{1,0:T(8,128)(2,1)S(1)} %slice.29), channel_id=1, source_target_pairs={{0,24},{8,0},{16,8},{24,16},{2,26},{10,2},{18,10},{26,18},{4,28},{... | collective-permute-start | bytes 491528 | tf_op jit(solution)/shard_map/ppermute | solution.py:49
  22.9 6.6 %collective-permute-start.5 = (bf16[32,2560]{1,0:T(8,128)(2,1)S(1)}, bf16[32,2560]{1,0:T(8,128)(2,1)S(1)}, u32[]{:S(2)}, u32[]{:S(2)}) collective-permute-start(bf16[32,2560]{1,0:T(8,128)(2,1)S(1)} %slice.28), channel_id=1, source_target_pairs={{0,8},{8,16},{16,24},{24,0},{2,10},{10,18},{18,26},{26,2},{4,12},{... | collective-permute-start | bytes 491528 | tf_op jit(solution)/shard_map/ppermute | solution.py:49
  29.6 4.4 %collective-permute-start.14 = (bf16[128,1536]{1,0:T(8,128)(2,1)S(1)}, bf16[128,1536]{1,0:T(8,128)(2,1)S(1)}, u32[]{:S(2)}, u32[]{:S(2)}) collective-permute-start(bf16[128,1536]{1,0:T(8,128)(2,1)S(1)} %slice.24.refs_1_), channel_id=1, source_target_pairs={{0,1},{1,0},{2,3},{3,2},{4,5},{5,4},{6,7},{7,6},{8,9},{9,8},{10,11... | collective-permute-start | bytes 1179656 | tf_op jit(solution)/shard_map/ppermute | solution.py:61
  29.7 9.4 %collective-permute-start.10 = (bf16[128,1536]{1,0:T(8,128)(2,1)S(1)}, bf16[128,1536]{1,0:T(8,128)(2,1)S(1)}, u32[]{:S(2)}, u32[]{:S(2)}) collective-permute-start(bf16[128,1536]{1,0:T(8,128)(2,1)S(1)} %slice.24.refs_1_), channel_id=1, source_target_pairs={{0,96},{32,0},{64,32},{96,64},{2,98},{34,2},{66,34},{98,66},{4,100... | collective-permute-start | bytes 1179656 | tf_op jit(solution)/shard_map/ppermute | solution.py:49
  33.8 9.0 %collective-permute-start.8 = (bf16[128,1536]{1,0:T(8,128)(2,1)S(1)}, bf16[128,1536]{1,0:T(8,128)(2,1)S(1)}, u32[]{:S(2)}, u32[]{:S(2)}) collective-permute-start(bf16[128,1536]{1,0:T(8,128)(2,1)S(1)} %slice.24.refs_1_), channel_id=1, source_target_pairs={{0,32},{32,64},{64,96},{96,0},{2,34},{34,66},{66,98},{98,2},{4,36}... | collective-permute-start | bytes 1179656 | tf_op jit(solution)/shard_map/ppermute | solution.py:49
  33.9 13.2 %collective-permute-start.7 = (bf16[128,1536]{1,0:T(8,128)(2,1)S(1)}, bf16[128,1536]{1,0:T(8,128)(2,1)S(1)}, u32[]{:S(2)}, u32[]{:S(2)}) collective-permute-start(bf16[128,1536]{1,0:T(8,128)(2,1)S(1)} %slice.23.refs_0_), channel_id=1, source_target_pairs={{0,32},{32,64},{64,96},{96,0},{2,34},{34,66},{66,98},{98,2},{4,36}... | collective-permute-start | bytes 1179656 | tf_op jit(solution)/shard_map/ppermute | solution.py:49
  33.9 13.1 %collective-permute-start.13 = (bf16[128,1536]{1,0:T(8,128)(2,1)S(1)}, bf16[128,1536]{1,0:T(8,128)(2,1)S(1)}, u32[]{:S(2)}, u32[]{:S(2)}) collective-permute-start(bf16[128,1536]{1,0:T(8,128)(2,1)S(1)} %slice.23.refs_0_), channel_id=1, source_target_pairs={{0,1},{1,0},{2,3},{3,2},{4,5},{5,4},{6,7},{7,6},{8,9},{9,8},{10,11... | collective-permute-start | bytes 1179656 | tf_op jit(solution)/shard_map/ppermute | solution.py:61
  34.0 13.0 %collective-permute-start.9 = (bf16[128,1536]{1,0:T(8,128)(2,1)S(1)}, bf16[128,1536]{1,0:T(8,128)(2,1)S(1)}, u32[]{:S(2)}, u32[]{:S(2)}) collective-permute-start(bf16[128,1536]{1,0:T(8,128)(2,1)S(1)} %slice.23.refs_0_), channel_id=1, source_target_pairs={{0,96},{32,0},{64,32},{96,64},{2,98},{34,2},{66,34},{98,66},{4,100... | collective-permute-start | bytes 1179656 | tf_op jit(solution)/shard_map/ppermute | solution.py:49
  39.1 8.4 %collective-permute-start.18 = (bf16[128,1536]{1,0:T(8,128)(2,1)S(1)}, bf16[128,1536]{1,0:T(8,128)(2,1)S(1)}, u32[]{:S(2)}, u32[]{:S(2)}) collective-permute-start(bf16[128,1536]{1,0:T(8,128)(2,1)S(1)} %collective-permute-done.10.refs_5_), channel_id=1, source_target_pairs={{0,1},{1,0},{2,3},{3,2},{4,5},{5,4},{6,7},{7,6},{8,9},{9,8},{10,11... | collective-permute-start | bytes 1179656 | tf_op jit(solution)/shard_map/ppermute | solution.py:61
  42.8 7.8 %collective-permute-start.12 = (bf16[128,1536]{1,0:T(8,128)(2,1)S(1)}, bf16[128,1536]{1,0:T(8,128)(2,1)S(1)}, u32[]{:S(2)}, u32[]{:S(2)}) collective-permute-start(bf16[128,1536]{1,0:T(8,128)(2,1)S(1)} %collective-permute-done.10.refs_5_), channel_id=1, source_target_pairs={{0,96},{32,0},{64,32},{96,64},{2,98},{34,2},{66,34},{98,66},{4,100... | collective-permute-start | bytes 1179656 | tf_op jit(solution)/shard_map/ppermute | solution.py:49
  47.0 9.0 %collective-permute-start.11 = (bf16[128,1536]{1,0:T(8,128)(2,1)S(1)}, bf16[128,1536]{1,0:T(8,128)(2,1)S(1)}, u32[]{:S(2)}, u32[]{:S(2)}) collective-permute-start(bf16[128,1536]{1,0:T(8,128)(2,1)S(1)} %collective-permute-done.7.refs_2_), channel_id=1, source_target_pairs={{0,32},{32,64},{64,96},{96,0},{2,34},{34,66},{66,98},{98,2},{4,36}... | collective-permute-start | bytes 1179656 | tf_op jit(solution)/shard_map/ppermute | solution.py:49
  47.0 9.0 %collective-permute-start.15 = (bf16[128,1536]{1,0:T(8,128)(2,1)S(1)}, bf16[128,1536]{1,0:T(8,128)(2,1)S(1)}, u32[]{:S(2)}, u32[]{:S(2)}) collective-permute-start(bf16[128,1536]{1,0:T(8,128)(2,1)S(1)} %collective-permute-done.7.refs_2_), channel_id=1, source_target_pairs={{0,1},{1,0},{2,3},{3,2},{4,5},{5,4},{6,7},{7,6},{8,9},{9,8},{10,11... | collective-permute-start | bytes 1179656 | tf_op jit(solution)/shard_map/ppermute | solution.py:61
  47.1 9.0 %collective-permute-start.16 = (bf16[128,1536]{1,0:T(8,128)(2,1)S(1)}, bf16[128,1536]{1,0:T(8,128)(2,1)S(1)}, u32[]{:S(2)}, u32[]{:S(2)}) collective-permute-start(bf16[128,1536]{1,0:T(8,128)(2,1)S(1)} %collective-permute-done.8.refs_3_), channel_id=1, source_target_pairs={{0,1},{1,0},{2,3},{3,2},{4,5},{5,4},{6,7},{7,6},{8,9},{9,8},{10,11... | collective-permute-start | bytes 1179656 | tf_op jit(solution)/shard_map/ppermute | solution.py:61
  47.6 8.5 %collective-permute-start.17 = (bf16[128,1536]{1,0:T(8,128)(2,1)S(1)}, bf16[128,1536]{1,0:T(8,128)(2,1)S(1)}, u32[]{:S(2)}, u32[]{:S(2)}) collective-permute-start(bf16[128,1536]{1,0:T(8,128)(2,1)S(1)} %collective-permute-done.9.refs_4_), channel_id=1, source_target_pairs={{0,1},{1,0},{2,3},{3,2},{4,5},{5,4},{6,7},{7,6},{8,9},{9,8},{10,11... | collective-permute-start | bytes 1179656 | tf_op jit(solution)/shard_map/ppermute | solution.py:61
  50.6 5.4 %collective-permute-start.20 = (bf16[128,1536]{1,0:T(8,128)(2,1)S(1)}, bf16[128,1536]{1,0:T(8,128)(2,1)S(1)}, u32[]{:S(2)}, u32[]{:S(2)}) collective-permute-start(bf16[128,1536]{1,0:T(8,128)(2,1)S(1)} %collective-permute-done.12.refs_7_), channel_id=1, source_target_pairs={{0,1},{1,0},{2,3},{3,2},{4,5},{5,4},{6,7},{7,6},{8,9},{9,8},{10,11... | collective-permute-start | bytes 1179656 | tf_op jit(solution)/shard_map/ppermute | solution.py:61
  56.0 1.7 %collective-permute-start.19 = (bf16[128,1536]{1,0:T(8,128)(2,1)S(1)}, bf16[128,1536]{1,0:T(8,128)(2,1)S(1)}, u32[]{:S(2)}, u32[]{:S(2)}) collective-permute-start(bf16[128,1536]{1,0:T(8,128)(2,1)S(1)} %collective-permute-done.11.refs_6_), channel_id=1, source_target_pairs={{0,1},{1,0},{2,3},{3,2},{4,5},{5,4},{6,7},{7,6},{8,9},{9,8},{10,11... | collective-permute-start | bytes 1179656 | tf_op jit(solution)/shard_map/ppermute | solution.py:61
  62.6 15.1 %all-to-all-start = ((bf16[4,384,384]{2,1,0:T(8,128)(2,1)}), bf16[4,384,384]{2,1,0:T(8,128)(2,1)S(1)}, u32[]{:S(2)}, u32[]{:S(2)}) async-start(bf16[4,384,384]{2,1,0:T(8,128)(2,1)} %project.1), calls=%async_computation | async-start | bytes 2359296 | tf_op jit(solution)/shard_map/all_to_all | solution.py:389
  77.8 20.8 %collective-permute-start.22 = (bf16[4,128,384]{2,1,0:T(8,128)(2,1)S(1)}, bf16[4,128,384]{2,1,0:T(8,128)(2,1)S(1)}, u32[]{:S(2)}, u32[]{:S(2)}) collective-permute-start(bf16[4,128,384]{2,1,0:T(8,128)(2,1)S(1)} %slice.27), channel_id=1, source_target_pairs={{0,96},{32,64},{64,32},{96,0},{2,98},{34,66},{66,34},{98,2},{4,100... | collective-permute-start | bytes 1179656 | tf_op jit(solution)/shard_map/ppermute | solution.py:57
  77.9 20.7 %collective-permute-start.21 = (bf16[4,128,384]{2,1,0:T(8,128)(2,1)S(1)}, bf16[4,128,384]{2,1,0:T(8,128)(2,1)S(1)}, u32[]{:S(2)}, u32[]{:S(2)}) collective-permute-start(bf16[4,128,384]{2,1,0:T(8,128)(2,1)S(1)} %slice.27), channel_id=1, source_target_pairs={{0,32},{32,0},{64,96},{96,64},{2,34},{34,2},{66,98},{98,66},{4,36}... | collective-permute-start | bytes 1179656 | tf_op jit(solution)/shard_map/ppermute | solution.py:57
  78.0 42.4 %collective-permute-start.24 = (bf16[256,1024]{1,0:T(8,128)(2,1)S(1)}, bf16[256,1024]{1,0:T(8,128)(2,1)S(1)}, u32[]{:S(2)}, u32[]{:S(2)}) collective-permute-start(bf16[256,1024]{1,0:T(8,128)(2,1)S(1)} %pad_maximum_fusion.1), channel_id=1, source_target_pairs={{0,32},{32,0},{64,96},{96,64},{2,34},{34,2},{66,98},{98,66},{4,36}... | collective-permute-start | bytes 1572872 | tf_op jit(solution)/shard_map/ppermute | solution.py:57
  98.6 21.8 %collective-permute-start.23 = (bf16[4,128,384]{2,1,0:T(8,128)(2,1)S(1)}, bf16[4,128,384]{2,1,0:T(8,128)(2,1)S(1)}, u32[]{:S(2)}, u32[]{:S(2)}) collective-permute-start(bf16[4,128,384]{2,1,0:T(8,128)(2,1)S(1)} %collective-permute-done.21.refs_0_), channel_id=1, source_target_pairs={{0,96},{32,64},{64,32},{96,0},{2,98},{34,66},{66,34},{98,2},{4,100... | collective-permute-start | bytes 1179656 | tf_op jit(solution)/shard_map/ppermute | solution.py:57
  120.5 36.1 %collective-permute-start.26 = (bf16[512,1024]{1,0:T(8,128)(2,1)S(1)}, bf16[512,1024]{1,0:T(8,128)(2,1)S(1)}, u32[]{:S(2)}, u32[]{:S(2)}) collective-permute-start(bf16[512,1024]{1,0:T(8,128)(2,1)S(1)} %constant_dynamic-update-slice_fusion.5.refs_4_), channel_id=1, source_target_pairs={{0,96},{32,64},{64,32},{96,0},{2,98},{34,66},{66,34},{98,2},{4,100... | collective-permute-start | bytes 3145736 | tf_op jit(solution)/shard_map/ppermute | solution.py:57
  120.6 27.1 %collective-permute-start.25 = (bf16[512,1024]{1,0:T(8,128)(2,1)S(1)}, bf16[512,1024]{1,0:T(8,128)(2,1)S(1)}, u32[]{:S(2)}, u32[]{:S(2)}) collective-permute-start(bf16[512,1024]{1,0:T(8,128)(2,1)S(1)} %constant_dynamic-update-slice_fusion.5.refs_4_), channel_id=1, source_target_pairs={{0,1},{1,0},{2,3},{3,2},{4,5},{5,4},{6,7},{7,6},{8,9},{9,8},{10,11... | collective-permute-start | bytes 3145736 | tf_op jit(solution)/shard_map/ppermute | solution.py:61
  156.6 11.0 %collective-permute-start.30 = (bf16[512,1024]{1,0:T(8,128)(2,1)S(1)}, bf16[512,1024]{1,0:T(8,128)(2,1)S(1)}, u32[]{:S(2)}, u32[]{:S(2)}) collective-permute-start(bf16[512,1024]{1,0:T(8,128)(2,1)S(1)} %collective-permute-done.26.refs_5_), channel_id=1, source_target_pairs={{0,1},{1,0},{2,3},{3,2},{4,5},{5,4},{6,7},{7,6},{8,9},{9,8},{10,11... | collective-permute-start | bytes 3145736 | tf_op jit(solution)/shard_map/ppermute | solution.py:61
  157.2 6.9 %collective-permute-start.27 = (bf16[256,384]{1,0:T(8,128)(2,1)S(1)}, bf16[256,384]{1,0:T(8,128)(2,1)S(1)}, u32[]{:S(2)}, u32[]{:S(2)}) collective-permute-start(bf16[256,384]{1,0:T(8,128)(2,1)S(1)} %get-tuple-element.64), channel_id=1, source_target_pairs={{0,8},{8,16},{16,24},{24,0},{2,10},{10,18},{18,26},{26,2},{4,12},{... | collective-permute-start | bytes 589832 | tf_op jit(solution)/shard_map/ppermute | solution.py:49
  157.7 8.0 %collective-permute-start.28 = (bf16[256,384]{1,0:T(8,128)(2,1)S(1)}, bf16[256,384]{1,0:T(8,128)(2,1)S(1)}, u32[]{:S(2)}, u32[]{:S(2)}) collective-permute-start(bf16[256,384]{1,0:T(8,128)(2,1)S(1)} %get-tuple-element.65), channel_id=1, source_target_pairs={{0,24},{8,0},{16,8},{24,16},{2,26},{10,2},{18,10},{26,18},{4,28},{... | collective-permute-start | bytes 589832 | tf_op jit(solution)/shard_map/ppermute | solution.py:49
  160.4 7.2 %collective-permute-start.29 = (bf16[256,384]{1,0:T(8,128)(2,1)S(1)}, bf16[256,384]{1,0:T(8,128)(2,1)S(1)}, u32[]{:S(2)}, u32[]{:S(2)}) collective-permute-start(bf16[256,384]{1,0:T(8,128)(2,1)S(1)} %get-tuple-element.66), channel_id=1, source_target_pairs={{0,16},{8,24},{16,0},{24,8},{2,18},{10,26},{18,2},{26,10},{4,20},{... | collective-permute-start | bytes 589832 | tf_op jit(solution)/shard_map/ppermute | solution.py:49
  (3 other events, 104.0 us)

commit v2 on v1

--- a/solution.py
+++ b/solution.py
@@ -402,19 +402,20 @@
     sums = attend(every, q_row, k_row, qkv, [qkv], None, False)
     sums, kv_near, kv_next = lax.optimization_barrier((sums, kv_near, kv_next))
     kv_far = pair(kv_near, OUTER, True)
-    sums = attend(every, q_row, k_row, qkv, [kv_near], sums, False)
+    first_sums = sums
+    sums = attend(away, q_row, k_row, qkv, [kv_near], sums, False)
     sums, kv_next, kv_far, out_near = lax.optimization_barrier((sums, kv_next, kv_far, out_near))
     out_half = jnp.concatenate([out_own, out_near], axis=0)
     out_other = pair(out_half, OUTER, True)
     out_half_theirs = swap(out_half)
     behind, ahead, across = attend(away, q_row, k_row, qkv, [kv_next, kv_far], sums, True)
-    sums, kv_next, kv_far, behind, ahead, across, out_half_theirs = lax.optimization_barrier(
-        (sums, kv_next, kv_far, behind, ahead, across, out_half_theirs)
+    first_sums, kv_next, kv_far, behind, ahead, across, out_half_theirs = lax.optimization_barrier(
+        (first_sums, kv_next, kv_far, behind, ahead, across, out_half_theirs)
     )
     across = shift(across, INNER, 2)
     ahead = shift(ahead, INNER, 1)
     behind = shift(behind, INNER, -1)
-    (own,) = attend(here.reshape(1), q_row, k_row, qkv, [kv_next, kv_far], sums, True)
+    (own,) = attend(here.reshape(1), q_row, k_row, qkv, [kv_near, kv_next, kv_far], first_sums, True)
     own, out_other = lax.optimization_barrier((own, out_other))
     out_other_theirs = swap(out_other)
     return mix(

time: 172 us -> 173 us (level)
  starting transfers between devices: 33.5 us -> 40.5 us
  waiting for transfers between devices: 53.5 us -> 48.6 us
    ppermute x16, waiting for transfers between devices: 40.5 us -> 35 us  [shift(): return lax.ppermute(array, AXES, shift_pairs(axis_of_core, step))]
    ppermute x16, starting transfers between devices: 22.8 us -> 26.8 us  [shift(): return lax.ppermute(array, AXES, shift_pairs(axis_of_core, step))]
    ppermute x5, starting transfers between devices: 5.58 us -> 8.58 us  [pair(): return lax.ppermute(array, AXES, pairs)]
  transfers between devices with their start and end apart: 32 -> 32, of which waited for: 14 -> 15; matrix products, arithmetic and copies ran while one was open for 0% -> 0% of each run, Pallas kernels for 42% -> 42%
where the time goes in v2:
time: 173 us
  Pallas kernels  81.2 us (47%)
  waiting for transfers between devices  48.6 us (28%)
  starting transfers between devices  40.5 us (23%)
  other arithmetic  2.17 us (1%)
    pallas_call x4, Pallas kernels, attend(): pl.pallas_call(kern, grid_spec=pltpu.PrefetchScalarGridSpec(num_scalar_pr...  72.4 us
    ppermute x16, waiting for transfers between devices, shift(): return lax.ppermute(array, AXES, shift_pairs(axis_of_core, step))  35 us
    ppermute x16, starting transfers between devices, shift(): return lax.ppermute(array, AXES, shift_pairs(axis_of_core, step))  26.8 us
    all_to_all x1, waiting for transfers between devices, per_device(): lax.all_to_all(qkv, AXES, split_axis=0, concat_axis=0, tiled=True, axis_i...  11.3 us
    ppermute x5, starting transfers between devices, pair(): return lax.ppermute(array, AXES, pairs)  8.58 us
    pallas_call x1, Pallas kernels, project(): pl.pallas_call(kern, in_specs=[pl.BlockSpec(memory_space=pltpu.SMEM)] + [...  4.88 us
    pallas_call x1, Pallas kernels, mix(): pl.pallas_call(kern, in_specs=[pl.BlockSpec(memory_space=pltpu.SMEM), *[p...  3.9 us
    all_to_all x1, starting transfers between devices, per_device(): lax.all_to_all(qkv, AXES, split_axis=0, concat_axis=0, tiled=True, axis_i...  3.53 us
  transfers between devices with their start and end apart: 32, of which 15 were waited for; matrix products, arithmetic and copies ran while one was open for 0% of the time, Pallas kernels for 42%

profile of v2, /device:TPU:0, one launch (start us, length us, event | category | flops | bytes accessed | tf_op | source)
XLA Modules:
  0.0 173.1 jit_solution(8449039382921076282)
XLA Ops:
  0.8 1.8 %collective-permute-start = (bf16[16,2560]{1,0:T(8,128)(2,1)S(1)}, bf16[16,2560]{1,0:T(8,128)(2,1)S(1)}, u32[]{:S(2)}, u32[]{:S(2)}) collective-permute-start(bf16[16,2560]{1,0:T(8,128)(2,1)S(1)} %get-tuple-element.69), channel_id=1, source_target_pairs={{0,2},{2,4},{4,6},{6,0},{8,10},{10,12},{12,14},{14,8},{16,18},{18,... | collective-permute-start | bytes 245768 | tf_op jit(solution)/shard_map/ppermute | solution.py:49
  2.6 1.5 collective-permute-start.1
  4.1 2.1 %collective-permute-start.2 = (bf16[16,2560]{1,0:T(8,128)(2,1)S(1)}, bf16[16,2560]{1,0:T(8,128)(2,1)S(1)}, u32[]{:S(2)}, u32[]{:S(2)}) collective-permute-start(bf16[16,2560]{1,0:T(8,128)(2,1)S(1)} %get-tuple-element.69), channel_id=1, source_target_pairs={{0,4},{2,6},{4,0},{6,2},{8,12},{10,14},{12,8},{14,10},{16,20},{18,... | collective-permute-start | bytes 245768 | tf_op jit(solution)/shard_map/ppermute | solution.py:49
  7.3 2.8 %collective-permute-done.2 = bf16[16,2560]{1,0:T(8,128)(2,1)S(1)} collective-permute-done((bf16[16,2560]{1,0:T(8,128)(2,1)S(1)}, bf16[16,2560]{1,0:T(8,128)(2,1)S(1)}, u32[]{:S(2)}, u32[]{:S(2)}) %collective-permute-start.2) | collective-permute-done | bytes 81952 | tf_op jit(solution)/shard_map/ppermute | solution.py:49
  10.9 1.7 collective-permute-start.3
  12.6 1.6 collective-permute-start.4
  14.3 5.4 %collective-permute-done.4 = bf16[64,2560]{1,0:T(8,128)(2,1)S(1)} collective-permute-done((bf16[64,2560]{1,0:T(8,128)(2,1)S(1)}, bf16[64,2560]{1,0:T(8,128)(2,1)S(1)}, u32[]{:S(2)}, u32[]{:S(2)}) %collective-permute-start.4) | collective-permute-done | bytes 327712 | tf_op jit(solution)/shard_map/ppermute | solution.py:49
  19.7 2.9 %collective-permute-start.6 = (bf16[32,2560]{1,0:T(8,128)(2,1)S(1)}, bf16[32,2560]{1,0:T(8,128)(2,1)S(1)}, u32[]{:S(2)}, u32[]{:S(2)}) collective-permute-start(bf16[32,2560]{1,0:T(8,128)(2,1)S(1)} %slice.29), channel_id=1, source_target_pairs={{0,24},{8,0},{16,8},{24,16},{2,26},{10,2},{18,10},{26,18},{4,28},{... | collective-permute-start | bytes 491528 | tf_op jit(solution)/shard_map/ppermute | solution.py:49
  22.8 2.7 %collective-permute-done.6 = bf16[32,2560]{1,0:T(8,128)(2,1)S(1)} collective-permute-done((bf16[32,2560]{1,0:T(8,128)(2,1)S(1)}, bf16[32,2560]{1,0:T(8,128)(2,1)S(1)}, u32[]{:S(2)}, u32[]{:S(2)}) %collective-permute-start.6) | collective-permute-done | bytes 163872 | tf_op jit(solution)/shard_map/ppermute | solution.py:49
  25.4 3.8 %collective-permute-done.5 = bf16[32,2560]{1,0:T(8,128)(2,1)S(1)} collective-permute-done((bf16[32,2560]{1,0:T(8,128)(2,1)S(1)}, bf16[32,2560]{1,0:T(8,128)(2,1)S(1)}, u32[]{:S(2)}, u32[]{:S(2)}) %collective-permute-start.5) | collective-permute-done | bytes 163872 | tf_op jit(solution)/shard_map/ppermute | solution.py:49
  29.3 3.7 %collective-permute-start.7 = (bf16[128,1536]{1,0:T(8,128)(2,1)S(1)}, bf16[128,1536]{1,0:T(8,128)(2,1)S(1)}, u32[]{:S(2)}, u32[]{:S(2)}) collective-permute-start(bf16[128,1536]{1,0:T(8,128)(2,1)S(1)} %slice.23.refs_0_), channel_id=1, source_target_pairs={{0,32},{32,64},{64,96},{96,0},{2,34},{34,66},{66,98},{98,2},{4,36}... | collective-permute-start | bytes 1179656 | tf_op jit(solution)/shard_map/ppermute | solution.py:49
  33.0 2.2 %collective-permute-start.8 = (bf16[128,1536]{1,0:T(8,128)(2,1)S(1)}, bf16[128,1536]{1,0:T(8,128)(2,1)S(1)}, u32[]{:S(2)}, u32[]{:S(2)}) collective-permute-start(bf16[128,1536]{1,0:T(8,128)(2,1)S(1)} %slice.24.refs_1_), channel_id=1, source_target_pairs={{0,32},{32,64},{64,96},{96,0},{2,34},{34,66},{66,98},{98,2},{4,36}... | collective-permute-start | bytes 1179656 | tf_op jit(solution)/shard_map/ppermute | solution.py:49
  37.5 3.5 %collective-permute-done.7.refs_2_ = bf16[128,1536]{1,0:T(8,128)(2,1)S(1)} collective-permute-done((bf16[128,1536]{1,0:T(8,128)(2,1)S(1)}, bf16[128,1536]{1,0:T(8,128)(2,1)S(1)}, u32[]{:S(2)}, u32[]{:S(2)}) %collective-permute-start.7) | collective-permute-done | bytes 393248 | tf_op jit(solution)/shard_map/ppermute | solution.py:49
  41.0 4.2 %collective-permute-done.8.refs_3_ = bf16[128,1536]{1,0:T(8,128)(2,1)S(1)} collective-permute-done((bf16[128,1536]{1,0:T(8,128)(2,1)S(1)}, bf16[128,1536]{1,0:T(8,128)(2,1)S(1)}, u32[]{:S(2)}, u32[]{:S(2)}) %collective-permute-start.8) | collective-permute-done | bytes 393248 | tf_op jit(solution)/shard_map/ppermute | solution.py:49
  45.2 3.2 %collective-permute-start.12 = (bf16[128,1536]{1,0:T(8,128)(2,1)S(1)}, bf16[128,1536]{1,0:T(8,128)(2,1)S(1)}, u32[]{:S(2)}, u32[]{:S(2)}) collective-permute-start(bf16[128,1536]{1,0:T(8,128)(2,1)S(1)} %collective-permute-done.10.refs_5_), channel_id=1, source_target_pairs={{0,96},{32,0},{64,32},{96,64},{2,98},{34,2},{66,34},{98,66},{4,100... | collective-permute-start | bytes 1179656 | tf_op jit(solution)/shard_map/ppermute | solution.py:49
  49.1 5.1 %collective-permute-done.11.refs_6_ = bf16[128,1536]{1,0:T(8,128)(2,1)S(1)} collective-permute-done((bf16[128,1536]{1,0:T(8,128)(2,1)S(1)}, bf16[128,1536]{1,0:T(8,128)(2,1)S(1)}, u32[]{:S(2)}, u32[]{:S(2)}) %collective-permute-start.11) | collective-permute-done | bytes 393248 | tf_op jit(solution)/shard_map/ppermute | solution.py:49
  57.1 4.9 %project.1 = bf16[4,384,384]{2,1,0:T(8,128)(2,1)} custom-call(s32[4]{0:T(128)S(1)} %pad_add_fusion.where_ref, bf16[384,2048]{1,0:T(8,128)(2,1)S(1)} %bitcast.13, bf16[128,1536]{1,0:T(8,128)(2,1)S(1)} %slice.23.refs_0_, bf16[128,1536]{1,0:T(8,128)(2,1)S(1)} %slice.24.refs_1_, bf16[128,1536]{1,0:T(8,128)(2,1)S(1)} %collective-permute-done.7.refs_2_, ...), custom_call_target="tpu_custom_call" | custom-call | flops 2415919104 | bytes 6291456 | tf_op jit(solution)/shard_map/project/pallas_call | solution.py:150
  62.0 3.5 %all-to-all-start = ((bf16[4,384,384]{2,1,0:T(8,128)(2,1)}), bf16[4,384,384]{2,1,0:T(8,128)(2,1)S(1)}, u32[]{:S(2)}, u32[]{:S(2)}) async-start(bf16[4,384,384]{2,1,0:T(8,128)(2,1)} %project.1), calls=%async_computation | async-start | bytes 2359296 | tf_op jit(solution)/shard_map/all_to_all | solution.py:389
  65.7 11.3 %all-to-all-done.q_ref.refs_0_ = bf16[4,384,384]{2,1,0:T(8,128)(2,1)S(1)} async-done(((bf16[4,384,384]{2,1,0:T(8,128)(2,1)}), bf16[4,384,384]{2,1,0:T(8,128)(2,1)S(1)}, u32[]{:S(2)}, u32[]{:S(2)}) %all-to-all-start) | async-done | bytes 1179680 | tf_op jit(solution)/shard_map/all_to_all | solution.py:389
  77.2 3.6 %collective-permute-start.22 = (bf16[4,128,384]{2,1,0:T(8,128)(2,1)S(1)}, bf16[4,128,384]{2,1,0:T(8,128)(2,1)S(1)}, u32[]{:S(2)}, u32[]{:S(2)}) collective-permute-start(bf16[4,128,384]{2,1,0:T(8,128)(2,1)S(1)} %slice.27), channel_id=1, source_target_pairs={{0,96},{32,64},{64,32},{96,0},{2,98},{34,66},{66,34},{98,2},{4,100... | collective-permute-start | bytes 1179656 | tf_op jit(solution)/shard_map/ppermute | solution.py:57
  80.8 18.5 %shard_map.73 = (f32[4,80,1536]{2,1,0:T(8,128)S(1)}, f32[4,8,1536]{2,1,0:T(8,128)S(1)}) custom-call(s32[4]{0:T(128)S(1)} %iota.19.place_ref, f32[1,64]{1,0:T(1,128)S(1)} %bitcast.15, f32[1,64]{1,0:T(1,128)S(1)} %bitcast.20, bf16[4,384,384]{2,1,0:T(8,128)(2,1)S(1)} %all-to-all-done.q_ref.refs_0_, bf16[4,384,384]{2,1,0:T(8,128)(2,1)S(1)} %all-to-all-done.q_ref.refs_0_), custom_call_target="tpu_custom_call" | custom-call | flops 19327352832 | bytes 393216 | tf_op jit(solution)/shard_map/pallas_call | solution.py:275
  99.4 1.3 collective-permute-start.24
  101.4 14.1 %shard_map.74 = (f32[4,80,1536]{2,1,0:T(8,128)S(1)}, f32[4,8,1536]{2,1,0:T(8,128)S(1)}) custom-call(s32[3]{0:T(128)S(1)} %pad_add_fusion.1.place_ref, f32[1,64]{1,0:T(1,128)S(1)} %bitcast.16, f32[1,64]{1,0:T(1,128)S(1)} %bitcast.21, bf16[4,384,384]{2,1,0:T(8,128)(2,1)S(1)} %all-to-all-done.q_ref.refs_0_, ...), custom_call_target="tpu_custom_call" | custom-call | flops 14495514624 | bytes 393216 | tf_op jit(solution)/shard_map/pallas_call | solution.py:275
  115.6 2.9 %collective-permute-start.26 = (bf16[512,1024]{1,0:T(8,128)(2,1)S(1)}, bf16[512,1024]{1,0:T(8,128)(2,1)S(1)}, u32[]{:S(2)}, u32[]{:S(2)}) collective-permute-start(bf16[512,1024]{1,0:T(8,128)(2,1)S(1)} %constant_dynamic-update-slice_fusion.5.refs_4_), channel_id=1, source_target_pairs={{0,96},{32,64},{64,32},{96,0},{2,98},{34,66},{66,34},{98,2},{4,100... | collective-permute-start | bytes 3145736 | tf_op jit(solution)/shard_map/ppermute | solution.py:57
  118.6 26.9 %shard_map.75 = (bf16[256,384]{1,0:T(8,128)(2,1)S(1)}, bf16[256,384]{1,0:T(8,128)(2,1)S(1)}, bf16[256,384]{1,0:T(8,128)(2,1)S(1)}) custom-call(s32[3]{0:T(128)S(1)} %pad_add_fusion.1.place_ref, f32[1,64]{1,0:T(1,128)S(1)} %bitcast.17, f32[1,64]{1,0:T(1,128)S(1)} %bitcast.22, bf16[4,384,384]{2,1,0:T(8,128)(2,1)S(1)} %all-to-all-done.q_ref.refs_0_, ...), custom_call_target="tpu_custom_call" | custom-call | flops 28991029248 | bytes 786432 | tf_op jit(solution)/shard_map/pallas_call | solution.py:275
  145.4 12.9 %shard_map.76.refs_0_ = bf16[256,384]{1,0:T(8,128)(2,1)S(1)} custom-call(s32[1]{0:T(128)} %bitcast.5.place_ref, f32[1,64]{1,0:T(1,128)S(1)} %bitcast.18, f32[1,64]{1,0:T(1,128)S(1)} %bitcast.23, bf16[4,384,384]{2,1,0:T(8,128)(2,1)S(1)} %all-to-all-done.q_ref.refs_0_, bf16[4,128,384]{2,1,0:T(8,128)(2,1)S(1)} %collective-permute-done.21.refs_0_, ...), custom_call_target="tpu_custom_call" | custom-call | flops 14495514624 | bytes 1179648 | tf_op jit(solution)/shard_map/pallas_call | solution.py:275
  158.7 1.5 collective-permute-start.27
  160.3 1.8 %collective-permute-start.28 = (bf16[256,384]{1,0:T(8,128)(2,1)S(1)}, bf16[256,384]{1,0:T(8,128)(2,1)S(1)}, u32[]{:S(2)}, u32[]{:S(2)}) collective-permute-start(bf16[256,384]{1,0:T(8,128)(2,1)S(1)} %get-tuple-element.65), channel_id=1, source_target_pairs={{0,24},{8,0},{16,8},{24,16},{2,26},{10,2},{18,10},{26,18},{4,28},{... | collective-permute-start | bytes 589832 | tf_op jit(solution)/shard_map/ppermute | solution.py:49
  162.4 3.3 %collective-permute-done.27.refs_1_ = bf16[256,384]{1,0:T(8,128)(2,1)S(1)} collective-permute-done((bf16[256,384]{1,0:T(8,128)(2,1)S(1)}, bf16[256,384]{1,0:T(8,128)(2,1)S(1)}, u32[]{:S(2)}, u32[]{:S(2)}) %collective-permute-start.27) | collective-permute-done | bytes 196640 | tf_op jit(solution)/shard_map/ppermute | solution.py:49
  165.7 1.7 collective-permute-done.28.refs_2_
  167.4 1.8 %collective-permute-done.29.refs_3_ = bf16[256,384]{1,0:T(8,128)(2,1)S(1)} collective-permute-done((bf16[256,384]{1,0:T(8,128)(2,1)S(1)}, bf16[256,384]{1,0:T(8,128)(2,1)S(1)}, u32[]{:S(2)}, u32[]{:S(2)}) %collective-permute-start.29) | collective-permute-done | bytes 196640 | tf_op jit(solution)/shard_map/ppermute | solution.py:49
  169.2 3.9 %mix.1 = bf16[384,2048]{1,0:T(8,128)(2,1)} custom-call(s32[4]{0:T(128)S(1)} %pad_add_fusion.where_ref, bf16[256,384]{1,0:T(8,128)(2,1)S(1)} %shard_map.76.refs_0_, bf16[256,384]{1,0:T(8,128)(2,1)S(1)} %collective-permute-done.27.refs_1_, bf16[256,384]{1,0:T(8,128)(2,1)S(1)} %collective-permute-done.28.refs_2_, ...), custom_call_target="tpu_custom_call" | custom-call | flops 1610612736 | bytes 4194304 | tf_op jit(solution)/shard_map/mix/pallas_call | solution.py:329
  (68 shorter events, 10.6 us)
Async XLA Ops:
  0.8 5.8 %collective-permute-start = (bf16[16,2560]{1,0:T(8,128)(2,1)S(1)}, bf16[16,2560]{1,0:T(8,128)(2,1)S(1)}, u32[]{:S(2)}, u32[]{:S(2)}) collective-permute-start(bf16[16,2560]{1,0:T(8,128)(2,1)S(1)} %get-tuple-element.69), channel_id=1, source_target_pairs={{0,2},{2,4},{4,6},{6,0},{8,10},{10,12},{12,14},{14,8},{16,18},{18,... | collective-permute-start | bytes 245768 | tf_op jit(solution)/shard_map/ppermute | solution.py:49
  2.6 4.7 %collective-permute-start.1 = (bf16[16,2560]{1,0:T(8,128)(2,1)S(1)}, bf16[16,2560]{1,0:T(8,128)(2,1)S(1)}, u32[]{:S(2)}, u32[]{:S(2)}) collective-permute-start(bf16[16,2560]{1,0:T(8,128)(2,1)S(1)} %get-tuple-element.69), channel_id=1, source_target_pairs={{0,6},{2,0},{4,2},{6,4},{8,14},{10,8},{12,10},{14,12},{16,22},{18,... | collective-permute-start | bytes 245768 | tf_op jit(solution)/shard_map/ppermute | solution.py:49
  4.1 5.9 %collective-permute-start.2 = (bf16[16,2560]{1,0:T(8,128)(2,1)S(1)}, bf16[16,2560]{1,0:T(8,128)(2,1)S(1)}, u32[]{:S(2)}, u32[]{:S(2)}) collective-permute-start(bf16[16,2560]{1,0:T(8,128)(2,1)S(1)} %get-tuple-element.69), channel_id=1, source_target_pairs={{0,4},{2,6},{4,0},{6,2},{8,12},{10,14},{12,8},{14,10},{16,20},{18,... | collective-permute-start | bytes 245768 | tf_op jit(solution)/shard_map/ppermute | solution.py:49
  10.9 11.7 %collective-permute-start.3 = (bf16[64,2560]{1,0:T(8,128)(2,1)S(1)}, bf16[64,2560]{1,0:T(8,128)(2,1)S(1)}, u32[]{:S(2)}, u32[]{:S(2)}) collective-permute-start(bf16[64,2560]{1,0:T(8,128)(2,1)S(1)} %pad_maximum_fusion.2), channel_id=1, source_target_pairs={{0,8},{8,16},{16,24},{24,0},{2,10},{10,18},{18,26},{26,2},{4,12},{... | collective-permute-start | bytes 983048 | tf_op jit(solution)/shard_map/ppermute | solution.py:49
  12.6 7.1 %collective-permute-start.4 = (bf16[64,2560]{1,0:T(8,128)(2,1)S(1)}, bf16[64,2560]{1,0:T(8,128)(2,1)S(1)}, u32[]{:S(2)}, u32[]{:S(2)}) collective-permute-start(bf16[64,2560]{1,0:T(8,128)(2,1)S(1)} %pad_maximum_fusion.2), channel_id=1, source_target_pairs={{0,24},{8,0},{16,8},{24,16},{2,26},{10,2},{18,10},{26,18},{4,28},{... | collective-permute-start | bytes 983048 | tf_op jit(solution)/shard_map/ppermute | solution.py:49
  19.7 5.8 %collective-permute-start.6 = (bf16[32,2560]{1,0:T(8,128)(2,1)S(1)}, bf16[32,2560]{1,0:T(8,128)(2,1)S(1)}, u32[]{:S(2)}, u32[]{:S(2)}) collective-permute-start(bf16[32,2560]{1,0:T(8,128)(2,1)S(1)} %slice.29), channel_id=1, source_target_pairs={{0,24},{8,0},{16,8},{24,16},{2,26},{10,2},{18,10},{26,18},{4,28},{... | collective-permute-start | bytes 491528 | tf_op jit(solution)/shard_map/ppermute | solution.py:49
  22.6 6.6 %collective-permute-start.5 = (bf16[32,2560]{1,0:T(8,128)(2,1)S(1)}, bf16[32,2560]{1,0:T(8,128)(2,1)S(1)}, u32[]{:S(2)}, u32[]{:S(2)}) collective-permute-start(bf16[32,2560]{1,0:T(8,128)(2,1)S(1)} %slice.28), channel_id=1, source_target_pairs={{0,8},{8,16},{16,24},{24,0},{2,10},{10,18},{18,26},{26,2},{4,12},{... | collective-permute-start | bytes 491528 | tf_op jit(solution)/shard_map/ppermute | solution.py:49
  29.3 11.7 %collective-permute-start.7 = (bf16[128,1536]{1,0:T(8,128)(2,1)S(1)}, bf16[128,1536]{1,0:T(8,128)(2,1)S(1)}, u32[]{:S(2)}, u32[]{:S(2)}) collective-permute-start(bf16[128,1536]{1,0:T(8,128)(2,1)S(1)} %slice.23.refs_0_), channel_id=1, source_target_pairs={{0,32},{32,64},{64,96},{96,0},{2,34},{34,66},{66,98},{98,2},{4,36}... | collective-permute-start | bytes 1179656 | tf_op jit(solution)/shard_map/ppermute | solution.py:49
  33.0 12.2 %collective-permute-start.8 = (bf16[128,1536]{1,0:T(8,128)(2,1)S(1)}, bf16[128,1536]{1,0:T(8,128)(2,1)S(1)}, u32[]{:S(2)}, u32[]{:S(2)}) collective-permute-start(bf16[128,1536]{1,0:T(8,128)(2,1)S(1)} %slice.24.refs_1_), channel_id=1, source_target_pairs={{0,32},{32,64},{64,96},{96,0},{2,34},{34,66},{66,98},{98,2},{4,36}... | collective-permute-start | bytes 1179656 | tf_op jit(solution)/shard_map/ppermute | solution.py:49
  35.2 10.1 %collective-permute-start.10 = (bf16[128,1536]{1,0:T(8,128)(2,1)S(1)}, bf16[128,1536]{1,0:T(8,128)(2,1)S(1)}, u32[]{:S(2)}, u32[]{:S(2)}) collective-permute-start(bf16[128,1536]{1,0:T(8,128)(2,1)S(1)} %slice.24.refs_1_), channel_id=1, source_target_pairs={{0,96},{32,0},{64,32},{96,64},{2,98},{34,2},{66,34},{98,66},{4,100... | collective-permute-start | bytes 1179656 | tf_op jit(solution)/shard_map/ppermute | solution.py:49
  36.3 12.2 %collective-permute-start.9 = (bf16[128,1536]{1,0:T(8,128)(2,1)S(1)}, bf16[128,1536]{1,0:T(8,128)(2,1)S(1)}, u32[]{:S(2)}, u32[]{:S(2)}) collective-permute-start(bf16[128,1536]{1,0:T(8,128)(2,1)S(1)} %slice.23.refs_0_), channel_id=1, source_target_pairs={{0,96},{32,0},{64,32},{96,64},{2,98},{34,2},{66,34},{98,66},{4,100... | collective-permute-start | bytes 1179656 | tf_op jit(solution)/shard_map/ppermute | solution.py:49
  37.5 11.0 %collective-permute-start.13 = (bf16[128,1536]{1,0:T(8,128)(2,1)S(1)}, bf16[128,1536]{1,0:T(8,128)(2,1)S(1)}, u32[]{:S(2)}, u32[]{:S(2)}) collective-permute-start(bf16[128,1536]{1,0:T(8,128)(2,1)S(1)} %slice.23.refs_0_), channel_id=1, source_target_pairs={{0,1},{1,0},{2,3},{3,2},{4,5},{5,4},{6,7},{7,6},{8,9},{9,8},{10,11... | collective-permute-start | bytes 1179656 | tf_op jit(solution)/shard_map/ppermute | solution.py:61
  41.0 8.0 %collective-permute-start.14 = (bf16[128,1536]{1,0:T(8,128)(2,1)S(1)}, bf16[128,1536]{1,0:T(8,128)(2,1)S(1)}, u32[]{:S(2)}, u32[]{:S(2)}) collective-permute-start(bf16[128,1536]{1,0:T(8,128)(2,1)S(1)} %slice.24.refs_1_), channel_id=1, source_target_pairs={{0,1},{1,0},{2,3},{3,2},{4,5},{5,4},{6,7},{7,6},{8,9},{9,8},{10,11... | collective-permute-start | bytes 1179656 | tf_op jit(solution)/shard_map/ppermute | solution.py:61
  45.2 9.0 %collective-permute-start.11 = (bf16[128,1536]{1,0:T(8,128)(2,1)S(1)}, bf16[128,1536]{1,0:T(8,128)(2,1)S(1)}, u32[]{:S(2)}, u32[]{:S(2)}) collective-permute-start(bf16[128,1536]{1,0:T(8,128)(2,1)S(1)} %collective-permute-done.7.refs_2_), channel_id=1, source_target_pairs={{0,32},{32,64},{64,96},{96,0},{2,34},{34,66},{66,98},{98,2},{4,36}... | collective-permute-start | bytes 1179656 | tf_op jit(solution)/shard_map/ppermute | solution.py:49
  45.2 9.0 %collective-permute-start.12 = (bf16[128,1536]{1,0:T(8,128)(2,1)S(1)}, bf16[128,1536]{1,0:T(8,128)(2,1)S(1)}, u32[]{:S(2)}, u32[]{:S(2)}) collective-permute-start(bf16[128,1536]{1,0:T(8,128)(2,1)S(1)} %collective-permute-done.10.refs_5_), channel_id=1, source_target_pairs={{0,96},{32,0},{64,32},{96,64},{2,98},{34,2},{66,34},{98,66},{4,100... | collective-permute-start | bytes 1179656 | tf_op jit(solution)/shard_map/ppermute | solution.py:49
  48.5 6.3 %collective-permute-start.15 = (bf16[128,1536]{1,0:T(8,128)(2,1)S(1)}, bf16[128,1536]{1,0:T(8,128)(2,1)S(1)}, u32[]{:S(2)}, u32[]{:S(2)}) collective-permute-start(bf16[128,1536]{1,0:T(8,128)(2,1)S(1)} %collective-permute-done.7.refs_2_), channel_id=1, source_target_pairs={{0,1},{1,0},{2,3},{3,2},{4,5},{5,4},{6,7},{7,6},{8,9},{9,8},{10,11... | collective-permute-start | bytes 1179656 | tf_op jit(solution)/shard_map/ppermute | solution.py:61
  48.5 7.5 %collective-permute-start.18 = (bf16[128,1536]{1,0:T(8,128)(2,1)S(1)}, bf16[128,1536]{1,0:T(8,128)(2,1)S(1)}, u32[]{:S(2)}, u32[]{:S(2)}) collective-permute-start(bf16[128,1536]{1,0:T(8,128)(2,1)S(1)} %collective-permute-done.10.refs_5_), channel_id=1, source_target_pairs={{0,1},{1,0},{2,3},{3,2},{4,5},{5,4},{6,7},{7,6},{8,9},{9,8},{10,11... | collective-permute-start | bytes 1179656 | tf_op jit(solution)/shard_map/ppermute | solution.py:61
  49.0 5.8 %collective-permute-start.16 = (bf16[128,1536]{1,0:T(8,128)(2,1)S(1)}, bf16[128,1536]{1,0:T(8,128)(2,1)S(1)}, u32[]{:S(2)}, u32[]{:S(2)}) collective-permute-start(bf16[128,1536]{1,0:T(8,128)(2,1)S(1)} %collective-permute-done.8.refs_3_), channel_id=1, source_target_pairs={{0,1},{1,0},{2,3},{3,2},{4,5},{5,4},{6,7},{7,6},{8,9},{9,8},{10,11... | collective-permute-start | bytes 1179656 | tf_op jit(solution)/shard_map/ppermute | solution.py:61
  54.2 1.7 collective-permute-start.17
  54.2 2.3 %collective-permute-start.19 = (bf16[128,1536]{1,0:T(8,128)(2,1)S(1)}, bf16[128,1536]{1,0:T(8,128)(2,1)S(1)}, u32[]{:S(2)}, u32[]{:S(2)}) collective-permute-start(bf16[128,1536]{1,0:T(8,128)(2,1)S(1)} %collective-permute-done.11.refs_6_), channel_id=1, source_target_pairs={{0,1},{1,0},{2,3},{3,2},{4,5},{5,4},{6,7},{7,6},{8,9},{9,8},{10,11... | collective-permute-start | bytes 1179656 | tf_op jit(solution)/shard_map/ppermute | solution.py:61
  54.7 2.3 %collective-permute-start.20 = (bf16[128,1536]{1,0:T(8,128)(2,1)S(1)}, bf16[128,1536]{1,0:T(8,128)(2,1)S(1)}, u32[]{:S(2)}, u32[]{:S(2)}) collective-permute-start(bf16[128,1536]{1,0:T(8,128)(2,1)S(1)} %collective-permute-done.12.refs_7_), channel_id=1, source_target_pairs={{0,1},{1,0},{2,3},{3,2},{4,5},{5,4},{6,7},{7,6},{8,9},{9,8},{10,11... | collective-permute-start | bytes 1179656 | tf_op jit(solution)/shard_map/ppermute | solution.py:61
  62.0 15.1 %all-to-all-start = ((bf16[4,384,384]{2,1,0:T(8,128)(2,1)}), bf16[4,384,384]{2,1,0:T(8,128)(2,1)S(1)}, u32[]{:S(2)}, u32[]{:S(2)}) async-start(bf16[4,384,384]{2,1,0:T(8,128)(2,1)} %project.1), calls=%async_computation | async-start | bytes 2359296 | tf_op jit(solution)/shard_map/all_to_all | solution.py:389
  77.1 23.6 %collective-permute-start.21 = (bf16[4,128,384]{2,1,0:T(8,128)(2,1)S(1)}, bf16[4,128,384]{2,1,0:T(8,128)(2,1)S(1)}, u32[]{:S(2)}, u32[]{:S(2)}) collective-permute-start(bf16[4,128,384]{2,1,0:T(8,128)(2,1)S(1)} %slice.27), channel_id=1, source_target_pairs={{0,32},{32,0},{64,96},{96,64},{2,34},{34,2},{66,98},{98,66},{4,36}... | collective-permute-start | bytes 1179656 | tf_op jit(solution)/shard_map/ppermute | solution.py:57
  77.2 23.4 %collective-permute-start.22 = (bf16[4,128,384]{2,1,0:T(8,128)(2,1)S(1)}, bf16[4,128,384]{2,1,0:T(8,128)(2,1)S(1)}, u32[]{:S(2)}, u32[]{:S(2)}) collective-permute-start(bf16[4,128,384]{2,1,0:T(8,128)(2,1)S(1)} %slice.27), channel_id=1, source_target_pairs={{0,96},{32,64},{64,32},{96,0},{2,98},{34,66},{66,34},{98,2},{4,100... | collective-permute-start | bytes 1179656 | tf_op jit(solution)/shard_map/ppermute | solution.py:57
  99.4 16.1 %collective-permute-start.24 = (bf16[256,1024]{1,0:T(8,128)(2,1)S(1)}, bf16[256,1024]{1,0:T(8,128)(2,1)S(1)}, u32[]{:S(2)}, u32[]{:S(2)}) collective-permute-start(bf16[256,1024]{1,0:T(8,128)(2,1)S(1)} %pad_maximum_fusion.1), channel_id=1, source_target_pairs={{0,32},{32,0},{64,96},{96,64},{2,34},{34,2},{66,98},{98,66},{4,36}... | collective-permute-start | bytes 1572872 | tf_op jit(solution)/shard_map/ppermute | solution.py:57
  100.7 14.8 %collective-permute-start.23 = (bf16[4,128,384]{2,1,0:T(8,128)(2,1)S(1)}, bf16[4,128,384]{2,1,0:T(8,128)(2,1)S(1)}, u32[]{:S(2)}, u32[]{:S(2)}) collective-permute-start(bf16[4,128,384]{2,1,0:T(8,128)(2,1)S(1)} %collective-permute-done.21.refs_0_), channel_id=1, source_target_pairs={{0,96},{32,64},{64,32},{96,0},{2,98},{34,66},{66,34},{98,2},{4,100... | collective-permute-start | bytes 1179656 | tf_op jit(solution)/shard_map/ppermute | solution.py:57
  115.5 29.9 %collective-permute-start.25 = (bf16[512,1024]{1,0:T(8,128)(2,1)S(1)}, bf16[512,1024]{1,0:T(8,128)(2,1)S(1)}, u32[]{:S(2)}, u32[]{:S(2)}) collective-permute-start(bf16[512,1024]{1,0:T(8,128)(2,1)S(1)} %constant_dynamic-update-slice_fusion.5.refs_4_), channel_id=1, source_target_pairs={{0,1},{1,0},{2,3},{3,2},{4,5},{5,4},{6,7},{7,6},{8,9},{9,8},{10,11... | collective-permute-start | bytes 3145736 | tf_op jit(solution)/shard_map/ppermute | solution.py:61
  115.6 42.8 %collective-permute-start.26 = (bf16[512,1024]{1,0:T(8,128)(2,1)S(1)}, bf16[512,1024]{1,0:T(8,128)(2,1)S(1)}, u32[]{:S(2)}, u32[]{:S(2)}) collective-permute-start(bf16[512,1024]{1,0:T(8,128)(2,1)S(1)} %constant_dynamic-update-slice_fusion.5.refs_4_), channel_id=1, source_target_pairs={{0,96},{32,64},{64,32},{96,0},{2,98},{34,66},{66,34},{98,2},{4,100... | collective-permute-start | bytes 3145736 | tf_op jit(solution)/shard_map/ppermute | solution.py:57
  158.4 10.8 %collective-permute-start.30 = (bf16[512,1024]{1,0:T(8,128)(2,1)S(1)}, bf16[512,1024]{1,0:T(8,128)(2,1)S(1)}, u32[]{:S(2)}, u32[]{:S(2)}) collective-permute-start(bf16[512,1024]{1,0:T(8,128)(2,1)S(1)} %collective-permute-done.26.refs_5_), channel_id=1, source_target_pairs={{0,1},{1,0},{2,3},{3,2},{4,5},{5,4},{6,7},{7,6},{8,9},{9,8},{10,11... | collective-permute-start | bytes 3145736 | tf_op jit(solution)/shard_map/ppermute | solution.py:61
  158.7 6.9 %collective-permute-start.27 = (bf16[256,384]{1,0:T(8,128)(2,1)S(1)}, bf16[256,384]{1,0:T(8,128)(2,1)S(1)}, u32[]{:S(2)}, u32[]{:S(2)}) collective-permute-start(bf16[256,384]{1,0:T(8,128)(2,1)S(1)} %get-tuple-element.64), channel_id=1, source_target_pairs={{0,8},{8,16},{16,24},{24,0},{2,10},{10,18},{18,26},{26,2},{4,12},{... | collective-permute-start | bytes 589832 | tf_op jit(solution)/shard_map/ppermute | solution.py:49
  160.3 7.1 %collective-permute-start.28 = (bf16[256,384]{1,0:T(8,128)(2,1)S(1)}, bf16[256,384]{1,0:T(8,128)(2,1)S(1)}, u32[]{:S(2)}, u32[]{:S(2)}) collective-permute-start(bf16[256,384]{1,0:T(8,128)(2,1)S(1)} %get-tuple-element.65), channel_id=1, source_target_pairs={{0,24},{8,0},{16,8},{24,16},{2,26},{10,2},{18,10},{26,18},{4,28},{... | collective-permute-start | bytes 589832 | tf_op jit(solution)/shard_map/ppermute | solution.py:49
  162.1 7.2 %collective-permute-start.29 = (bf16[256,384]{1,0:T(8,128)(2,1)S(1)}, bf16[256,384]{1,0:T(8,128)(2,1)S(1)}, u32[]{:S(2)}, u32[]{:S(2)}) collective-permute-start(bf16[256,384]{1,0:T(8,128)(2,1)S(1)} %get-tuple-element.66), channel_id=1, source_target_pairs={{0,16},{8,24},{16,0},{24,8},{2,18},{10,26},{18,2},{26,10},{4,20},{... | collective-permute-start | bytes 589832 | tf_op jit(solution)/shard_map/ppermute | solution.py:49
  (3 other events, 103.0 us)
